TPU v7x, 32 devices: a whole 2x2x4 slice. The times are simulated.
32 devices in a mesh: sp: 8 (over z, y), tp: 4 (over x, core).
Axes of the slice: x: 2, y: 2, z: 4, core: 2. Of those that a mesh axis runs over, the one named last changes fastest.
Arguments:
- tokens: bfloat16 [2048, 2048], P(('sp', 'tp')), may hold values from -6 to 6
- norm_gain: float32 [2048], replicated, may hold values from 0.1 to 1.9
- ret_query: bfloat16 [2048, 1024], P('sp', 'tp'), may hold values from -0.125 to 0.125
- ret_key: bfloat16 [2048, 1024], P('sp', 'tp'), may hold values from -0.125 to 0.125
- ret_value: bfloat16 [2048, 2048], P('sp', 'tp'), may hold values from -0.125 to 0.125
- log_decay: float32 [8, 2048], P('tp', 'sp'), may hold values from -2 to 0, as said below
- att_query: bfloat16 [2048, 2048], P('sp', 'tp')
- att_key: bfloat16 [2048, 256], P('sp', 'tp')
- att_value: bfloat16 [2048, 256], P('sp', 'tp'), may hold values from -0.125 to 0.125
- sink_logits: float32 [32], P('tp'), may hold values from 3 to 6
- ret_out: bfloat16 [2048, 2048], P('tp', 'sp'), may hold values from -0.125 to 0.125
- att_out: bfloat16 [2048, 2048], P('tp', 'sp'), may hold values from -1 to 1
Outputs:
- mixed: bfloat16 [2048, 2048], P(('sp', 'tp'))
Inputs may be any that keep to these rules, and one draw needn't show every extreme that they name: `log_decay`: strictly negative.
All inputs are finite; a program needn't handle non-finite values.
Results may differ from a plain program's by a relative error of at most 0.013.
Values may be sent and summed in bfloat16 or wider, within the bound.
A program may use at most 128 MiB of HBM per device.

v0:
```python
import functools

import jax
import jax.numpy as jnp
from jax import lax
from jax.experimental import pallas as pl
from jax.experimental.pallas import tpu as pltpu
from jax.sharding import PartitionSpec as P

MESH = pl.DeviceIdType.MESH
LANES = 128

RETAIN_KEY_SIZE = 128
V_DIM = 256
HEAD_DIM = 64
WINDOW = 128
BLOCK = 128


epsilon = 1e-05
rope_base = 10000.0
masked_out = -1e30


def rotate(values, positions):
    half_dim = values.shape[-1] // 2
    inverse = rope_base ** (-jnp.arange(half_dim, dtype=jnp.float32) / half_dim)
    angles = positions.astype(jnp.float32)[:, None] * inverse[None, :]
    cosine = jnp.cos(angles)[:, None, :]
    sine_part = jnp.sin(angles)[:, None, :]
    first_half = values[..., :half_dim].astype(jnp.float32)
    second_half = values[..., half_dim:].astype(jnp.float32)
    return jnp.concatenate(
        [
            first_half * cosine - second_half * sine_part,
            second_half * cosine + first_half * sine_part,
        ],
        axis=-1,
    )


def retention_path(query_ret, key_ret, value_ret, log_decay, rim, logs, weights):
    tok_count, heads_here = (query_ret.shape[0], query_ret.shape[1])
    blocks = tok_count // BLOCK
    q_blocks = query_ret.reshape(blocks, BLOCK, heads_here, RETAIN_KEY_SIZE)
    k_blocks = key_ret.reshape(blocks, BLOCK, heads_here, RETAIN_KEY_SIZE)
    v_blocks = value_ret.reshape(blocks, BLOCK, heads_here, V_DIM)
    running = jnp.cumsum(log_decay.reshape(heads_here, blocks, BLOCK), axis=-1)
    closing = running[:, :, -1:]
    within = running[:, :, :, None] - running[:, :, None, :]
    causal_mask = jnp.arange(BLOCK)[:, None] >= jnp.arange(BLOCK)[None, :]
    weighting = jnp.where(causal_mask, jnp.exp(jnp.minimum(within, 0.0)), 0.0)
    scores = (
        jnp.einsum("nihd,njhd->hnij", q_blocks, k_blocks, preferred_element_type=jnp.float32)
        * weighting
    )
    in_block = jnp.einsum(
        "hnij,njhv->nihv", scores.astype(jnp.bfloat16), v_blocks, preferred_element_type=jnp.float32
    )
    key_fade = (
        k_blocks.astype(jnp.float32) * jnp.exp(closing - running).transpose(1, 2, 0)[..., None]
    ).astype(jnp.bfloat16)
    contrib = jnp.einsum("njhd,njhv->nhdv", key_fade, v_blocks, preferred_element_type=jnp.float32)
    block_fade = jnp.exp(closing[:, :, 0]).T

    def advance(carried, entry_pair):
        addend, factor = entry_pair
        return (carried * factor[:, None, None] + addend, carried)

    final_state, before = lax.scan(
        advance, jnp.zeros((heads_here, RETAIN_KEY_SIZE, V_DIM), jnp.float32), (contrib, block_fade)
    )
    n = lax.axis_size("sp")
    place = lax.axis_index("sp")
    before_rim, states, *wholes = exchange(
        rim, final_state.astype(jnp.bfloat16).reshape(2, -1, V_DIM), weights, n
    )
    states = states.reshape(n, heads_here, RETAIN_KEY_SIZE, V_DIM)
    spots = jnp.arange(n)
    between = (spots[None, :] > spots[:, None]) & (spots[None, :] < place)
    spans = jnp.sum(jnp.where(between[:, :, None], logs[None], 0.0), axis=1)
    shares = jnp.where((spots < place)[:, None], jnp.exp(spans), 0.0)
    arrived = jnp.sum(shares[:, :, None, None] * states.astype(jnp.float32), axis=0)
    leading = jnp.cumsum(closing[:, :, 0], axis=1) - closing[:, :, 0]
    before = before + arrived[None] * jnp.exp(leading).T[:, :, None, None]
    query_fade = (
        q_blocks.astype(jnp.float32) * jnp.exp(running).transpose(1, 2, 0)[..., None]
    ).astype(jnp.bfloat16)
    carried_term = jnp.einsum(
        "nihd,nhdv->nihv", query_fade.astype(jnp.float32), before, precision=lax.Precision.HIGHEST
    )
    final_product = in_block + carried_term
    final_product = final_product * lax.rsqrt(
        jnp.mean(final_product * final_product, axis=-1, keepdims=True) + epsilon
    )
    return final_product.reshape(tok_count, heads_here * V_DIM).astype(jnp.bfloat16), before_rim, wholes


def attention_path(query_att, stacked, window_rim, sink_logits, anchor):
    tok_count = query_att.shape[0]
    kv_here = stacked.shape[1] // (2 * HEAD_DIM)
    group_size = query_att.shape[1] // (kv_here * HEAD_DIM)
    blocks = tok_count // WINDOW
    extended = jnp.concatenate([window_rim, stacked], axis=0).reshape(
        blocks + 1, WINDOW, 2, kv_here, HEAD_DIM
    )
    paired = jnp.concatenate([extended[:-1], extended[1:]], axis=1)
    keys_pair = paired[:, :, 0]
    values_pair = paired[:, :, 1]
    q_blocks = query_att.reshape(blocks, WINDOW, kv_here, group_size, HEAD_DIM)
    scores = jnp.einsum(
        "nihgd,njhd->nhgij", q_blocks, keys_pair, preferred_element_type=jnp.float32
    ) * HEAD_DIM ** (-0.5)
    query_pos = anchor + (jnp.arange(blocks) * WINDOW)[:, None] + jnp.arange(WINDOW)[None, :]
    key_pos = (
        anchor + (jnp.arange(blocks) * WINDOW - WINDOW)[:, None] + jnp.arange(2 * WINDOW)[None, :]
    )
    allowed = (
        (key_pos[:, None, :] >= 0)
        & (key_pos[:, None, :] <= query_pos[:, :, None])
        & (query_pos[:, :, None] - key_pos[:, None, :] < WINDOW)
    )
    scores = jnp.where(allowed[:, None, None], scores, masked_out)
    sink_logit = sink_logits.reshape(kv_here, group_size)[None, :, :, None]
    highest = jnp.maximum(jnp.max(scores, axis=-1), sink_logit)
    lifted = jnp.exp(scores - highest[..., None])
    denominator = jnp.sum(lifted, axis=-1) + jnp.exp(sink_logit - highest)
    attn_weights = (lifted / denominator[..., None]).astype(jnp.bfloat16)
    final_product = jnp.einsum(
        "nhgij,njhd->nihgd", attn_weights, values_pair, preferred_element_type=jnp.float32
    )
    return final_product.reshape(tok_count, kv_here * group_size * HEAD_DIM).astype(jnp.bfloat16)


def ring_spot(index, count):
    half = count // 2
    return jnp.where(lax.rem(index, 2) == 0, index // 2, count - 1 - index // 2)


def ring_member(spot, count):
    half = count // 2
    return jnp.where(spot < half, 2 * spot, 2 * (count - 1 - spot) + 1)


def project_kernel(n, n_tp, normed_ref, pack_ref, log_ref, out_ref, logs_ref, rows_ref, held, total, sems, tok_sems):
    sp, tp = lax.axis_index("sp"), lax.axis_index("tp")
    depth, width = pack_ref.shape
    count = normed_ref.shape[0]
    half = n // 2
    spot = ring_spot(sp, n)
    ahead = ring_member(lax.rem(spot + 1, n), n)
    behind = ring_member(lax.rem(spot + n - 1, n), n)

    barrier = pltpu.get_barrier_semaphore()
    for peer in (ahead, behind):
        pl.semaphore_signal(barrier, inc=1, device_id=(peer, tp), device_id_type=MESH)
    for step in range(1, n_tp):
        pl.semaphore_signal(
            barrier, inc=1, device_id=(sp, lax.rem(tp + step, n_tp)), device_id_type=MESH
        )
    pl.semaphore_wait(barrier, 2 + n_tp - 1)

    def rows_of(member):
        return pl.ds(pl.multiple_of(member * depth, depth), depth)

    middle = (width // LANES + 1) // 2 * LANES
    spans = (pl.ds(0, middle), pl.ds(middle, width - middle))

    def owner(direction, distance):
        shift = n - distance if direction == 0 else distance
        return ring_member(lax.rem(spot + shift, n), n)

    def send(direction, step, part):
        member = owner(direction, step - 1)
        if part == 2:
            return pltpu.make_async_remote_copy(
                src_ref=log_ref if step == 1 else logs_ref.at[member],
                dst_ref=logs_ref.at[member],
                send_sem=sems.at[0, direction, step - 1, part],
                recv_sem=sems.at[1, direction, step - 1, part],
                device_id=(ahead if direction == 0 else behind, tp),
                device_id_type=MESH,
            )
        source = pack_ref.at[:, spans[part]] if step == 1 else held.at[rows_of(member), spans[part]]
        return pltpu.make_async_remote_copy(
            src_ref=source,
            dst_ref=held.at[rows_of(member), spans[part]],
            send_sem=sems.at[0, direction, step - 1, part],
            recv_sem=sems.at[1, direction, step - 1, part],
            device_id=(ahead if direction == 0 else behind, tp),
            device_id_type=MESH,
        )

    def arrival(direction, step, part):
        member = owner(direction, step)
        if part == 2:
            return pltpu.make_async_remote_copy(
                src_ref=log_ref,
                dst_ref=logs_ref.at[member],
                send_sem=sems.at[0, direction, step - 1, part],
                recv_sem=sems.at[1, direction, step - 1, part],
                device_id=(ahead if direction == 0 else behind, tp),
                device_id_type=MESH,
            )
        return pltpu.make_async_remote_copy(
            src_ref=held.at[rows_of(member), spans[part]],
            dst_ref=held.at[rows_of(member), spans[part]],
            send_sem=sems.at[0, direction, step - 1, part],
            recv_sem=sems.at[1, direction, step - 1, part],
            device_id=(ahead if direction == 0 else behind, tp),
            device_id_type=MESH,
        )

    started = []

    def go(copy):
        copy.start()
        started.append(copy)

    def parts_of(step, direction):
        first = direction
        if step == half:
            return (2, first) if direction == 0 else (first,)
        return (2, first, 1 - first)

    for slot in range(3):
        for direction in range(2):
            parts = parts_of(1, direction)
            if slot < len(parts):
                go(send(direction, 1, parts[slot]))
    tok_here = pl.ds(pl.multiple_of(tp * count, count), count)
    for step in range(1, n_tp):
        go(
            pltpu.make_async_remote_copy(
                src_ref=normed_ref,
                dst_ref=rows_ref.at[tok_here],
                send_sem=tok_sems.at[0, step - 1],
                recv_sem=tok_sems.at[1, step - 1],
                device_id=(sp, lax.rem(tp + step, n_tp)),
                device_id_type=MESH,
            )
        )
    rows_ref[tok_here, :] = normed_ref[...]
    logs_ref[sp] = log_ref[...]
    for step in range(1, n_tp):
        origin = pl.ds(pl.multiple_of(lax.rem(tp + n_tp - step, n_tp) * count, count), count)
        pltpu.make_async_remote_copy(
            src_ref=normed_ref,
            dst_ref=rows_ref.at[origin],
            send_sem=tok_sems.at[0, step - 1],
            recv_sem=tok_sems.at[1, step - 1],
            device_id=(sp, lax.rem(tp + step, n_tp)),
            device_id_type=MESH,
        ).wait_recv()

    blockwise = depth % LANES == 0

    def add(member, weights, first=False):
        columns = pl.ds(pl.multiple_of(member * depth, depth), depth)
        product = jnp.dot(rows_ref[:, columns], weights, preferred_element_type=jnp.float32)
        total[...] = product if first else total[...] + product

    if blockwise:
        add(sp, pack_ref[...], True)
    else:
        held[rows_of(sp), :] = pack_ref[...]
    for step in range(1, half + 1):
        for slot in range(3):
            for direction in range(2):
                parts = parts_of(step, direction)
                if slot < len(parts):
                    arrival(direction, step, parts[slot]).wait_recv()
                    if step < half and parts[slot] in parts_of(step + 1, direction):
                        go(send(direction, step + 1, parts[slot]))
        if blockwise:
            for direction in range(1 if step == half else 2):
                member = owner(direction, step)
                add(member, held[rows_of(member), :])
    if not blockwise:
        total[...] = jnp.dot(rows_ref[...], held[...], preferred_element_type=jnp.float32)
    out_ref[...] = total[...].astype(out_ref.dtype)
    for copy in started:
        copy.wait_send()


def project(normed, pack, logs, n, n_tp):
    depth, width = pack.shape
    count = normed.shape[0]
    features = normed.shape[1]
    vmem = pl.BlockSpec(memory_space=pltpu.VMEM)
    return pl.pallas_call(
        functools.partial(project_kernel, n, n_tp),
        out_shape=(
            jax.ShapeDtypeStruct((n_tp * count, width), jnp.bfloat16),
            jax.ShapeDtypeStruct((n,) + logs.shape, jnp.float32),
        ),
        in_specs=[vmem, vmem, vmem],
        out_specs=(vmem, vmem),
        scratch_shapes=[
            pltpu.VMEM((n_tp * count, features), jnp.bfloat16),
            pltpu.VMEM((n * depth, width), jnp.bfloat16),
            pltpu.VMEM((n_tp * count, width), jnp.float32),
            pltpu.SemaphoreType.DMA((2, 2, n // 2, 3)),
            pltpu.SemaphoreType.DMA((2, n_tp - 1)),
        ],
        compiler_params=pltpu.CompilerParams(
            collective_id=0, has_side_effects=True, vmem_limit_bytes=40 * 2**20
        ),
        cost_estimate=pl.CostEstimate(
            flops=400 * 2**30, bytes_accessed=n * depth * width * 2, transcendentals=0
        ),
        name="project_ring",
    )(normed, pack, logs)


def exchange_kernel(n, extra, rim_ref, state_ref, *refs):
    weight_refs = refs[:extra]
    before_ref, states_ref = refs[extra : extra + 2]
    whole_refs = refs[extra + 2 : 2 * extra + 2]
    sems, rim_sems = refs[2 * extra + 2 :]
    sources = [state_ref.at[0], state_ref.at[1], *weight_refs]
    sp, tp = lax.axis_index("sp"), lax.axis_index("tp")
    half = n // 2
    spot = ring_spot(sp, n)
    ahead = ring_member(lax.rem(spot + 1, n), n)
    behind = ring_member(lax.rem(spot + n - 1, n), n)
    later, earlier = lax.rem(sp + 1, n), lax.rem(sp + n - 1, n)
    barrier = pltpu.get_barrier_semaphore()
    for peer in (ahead, behind, later, earlier):
        pl.semaphore_signal(barrier, inc=1, device_id=(peer, tp), device_id_type=MESH)
    pl.semaphore_wait(barrier, 4)

    def owner(direction, distance):
        shift = n - distance if direction == 0 else distance
        return ring_member(lax.rem(spot + shift, n), n)

    def parts_of(step, direction):
        order = []
        for first in range(0, 2 + extra, 2):
            order.append(first + direction)
            if step < half:
                order.append(first + 1 - direction)
        return order

    def target(member, part):
        return states_ref.at[member, part] if part < 2 else whole_refs[part - 2].at[member]

    def hop(direction, step, part, member, source):
        return pltpu.make_async_remote_copy(
            src_ref=source,
            dst_ref=target(member, part),
            send_sem=sems.at[0, direction, step - 1, part],
            recv_sem=sems.at[1, direction, step - 1, part],
            device_id=(ahead if direction == 0 else behind, tp),
            device_id_type=MESH,
        )

    started = []
    rim = pltpu.make_async_remote_copy(
        src_ref=rim_ref,
        dst_ref=before_ref,
        send_sem=rim_sems.at[0],
        recv_sem=rim_sems.at[1],
        device_id=(later, tp),
        device_id_type=MESH,
    )
    for slot in range(2 + extra):
        for direction in range(2):
            parts = parts_of(1, direction)
            if slot < len(parts):
                copy = hop(direction, 1, parts[slot], sp, sources[parts[slot]])
                copy.start()
                started.append(copy)
    rim.start()
    states_ref[sp] = state_ref[...]
    for whole, piece in zip(whole_refs, weight_refs):
        whole[sp] = piece[...]
    for step in range(1, half + 1):
        for slot in range(2 + extra):
            for direction in range(2):
                parts = parts_of(step, direction)
                if slot < len(parts):
                    part = parts[slot]
                    member = owner(direction, step)
                    hop(direction, step, part, member, sources[part]).wait_recv()
                    if step < half and part in parts_of(step + 1, direction):
                        copy = hop(direction, step + 1, part, member, target(member, part))
                        copy.start()
                        started.append(copy)
    rim.wait()
    for copy in started:
        copy.wait_send()


def exchange(rim, state, weights, n):
    vmem = pl.BlockSpec(memory_space=pltpu.VMEM)
    return pl.pallas_call(
        functools.partial(exchange_kernel, n, len(weights)),
        out_shape=(
            jax.ShapeDtypeStruct(rim.shape, rim.dtype),
            jax.ShapeDtypeStruct((n,) + state.shape, state.dtype),
            *[jax.ShapeDtypeStruct((n,) + weight.shape, weight.dtype) for weight in weights],
        ),
        in_specs=[vmem] * (2 + len(weights)),
        out_specs=(vmem,) * (2 + len(weights)),
        scratch_shapes=[
            pltpu.SemaphoreType.DMA((2, 2, n // 2, 2 + len(weights))),
            pltpu.SemaphoreType.DMA((2,)),
        ],
        compiler_params=pltpu.CompilerParams(
            collective_id=2, has_side_effects=True, vmem_limit_bytes=40 * 2**20
        ),
        cost_estimate=pl.CostEstimate(
            flops=20 * 2**30, bytes_accessed=n * state.size * 2, transcendentals=0
        ),
        name="state_ring",
    )(rim, state, *weights)


def merge_kernel(n_tp, ret_ref, att_ref, ret_out_ref, att_out_ref, out_ref, total, outgoing, incoming, sent, landed, sems):
    sp, tp = lax.axis_index("sp"), lax.axis_index("tp")
    outer, inner = tp // 2, lax.rem(tp, 2)
    groups = n_tp // 2
    count = out_ref.shape[0]
    barrier = pltpu.get_barrier_semaphore()
    mate = outer * 2 + 1 - inner
    pl.semaphore_signal(barrier, inc=1, device_id=(sp, mate), device_id_type=MESH)
    for step in range(1, groups):
        peer = lax.rem(outer + step, groups) * 2 + inner
        pl.semaphore_signal(barrier, inc=1, device_id=(sp, peer), device_id_type=MESH)
    pl.semaphore_wait(barrier, groups)

    blocks, _, width = ret_out_ref.shape

    def partial(side, block):
        return jnp.dot(
            ret_ref[side], ret_out_ref[block], preferred_element_type=jnp.float32
        ) + jnp.dot(att_ref[side], att_out_ref[block], preferred_element_type=jnp.float32)

    for block in range(blocks):
        outgoing[:, block * width : (block + 1) * width] = partial(1 - inner, block).astype(
            jnp.bfloat16
        )
    swap = pltpu.make_async_remote_copy(
        src_ref=outgoing,
        dst_ref=incoming,
        send_sem=sems.at[0, 0],
        recv_sem=sems.at[1, 0],
        device_id=(sp, mate),
        device_id_type=MESH,
    )
    swap.start()
    for block in range(blocks):
        total[:, block * width : (block + 1) * width] = partial(inner, block)
    swap.wait_recv()
    own = total[...] + incoming[...].astype(jnp.float32)
    sent[...] = own.astype(jnp.bfloat16)
    copies = []
    for step in range(1, groups):
        other = lax.rem(outer + step, groups)
        copy = pltpu.make_async_remote_copy(
            src_ref=sent.at[pl.ds(pl.multiple_of(other * count, count), count)],
            dst_ref=landed.at[step - 1],
            send_sem=sems.at[0, step],
            recv_sem=sems.at[1, step],
            device_id=(sp, other * 2 + inner),
            device_id_type=MESH,
        )
        copy.start()
        copies.append(copy)
    mine = sent[pl.ds(pl.multiple_of(outer * count, count), count), :].astype(jnp.float32)
    for step, copy in enumerate(copies):
        copy.wait_recv()
        mine = mine + landed[step].astype(jnp.float32)
    out_ref[...] = mine.astype(out_ref.dtype)
    swap.wait_send()
    for copy in copies:
        copy.wait_send()


def merge(mixes, weights, n_tp):
    rows = mixes[0].shape[0]
    groups = n_tp // 2
    count = rows // n_tp
    width = weights[0].shape[0] * weights[0].shape[2]
    mixes = [
        mix.reshape(groups, 2, count, -1).transpose(1, 0, 2, 3).reshape(2, groups * count, -1)
        for mix in mixes
    ]
    vmem = pl.BlockSpec(memory_space=pltpu.VMEM)
    return pl.pallas_call(
        functools.partial(merge_kernel, n_tp),
        out_shape=jax.ShapeDtypeStruct((count, width), jnp.bfloat16),
        in_specs=[vmem] * 4,
        out_specs=vmem,
        scratch_shapes=[
            pltpu.VMEM((groups * count, width), jnp.float32),
            pltpu.VMEM((groups * count, width), jnp.bfloat16),
            pltpu.VMEM((groups * count, width), jnp.bfloat16),
            pltpu.VMEM((groups * count, width), jnp.bfloat16),
            pltpu.VMEM((max(1, groups - 1), count, width), jnp.bfloat16),
            pltpu.SemaphoreType.DMA((2, groups)),
        ],
        compiler_params=pltpu.CompilerParams(
            collective_id=1, has_side_effects=True, vmem_limit_bytes=40 * 2**20
        ),
        cost_estimate=pl.CostEstimate(
            flops=4 * rows * weights[0].size // 1, bytes_accessed=4 * weights[0].size, transcendentals=0
        ),
        name="merge_scatter",
    )(*mixes, *weights)


def on_device(
    tokens,
    norm_gain,
    ret_query,
    ret_key,
    ret_value,
    log_decay,
    att_query,
    att_key,
    att_value,
    sink_logits,
    ret_out,
    att_out,
):
    tok_float = tokens.astype(jnp.float32)
    normed = (
        tok_float
        * lax.rsqrt(jnp.mean(tok_float * tok_float, axis=-1, keepdims=True) + epsilon)
        * norm_gain
    ).astype(jnp.bfloat16)
    n, n_tp = lax.axis_size("sp"), lax.axis_size("tp")
    weights = (ret_query, ret_key, ret_value, att_query, att_key, att_value)
    widths = [weight.shape[1] for weight in weights]
    points = [sum(widths[:index]) for index in range(1, len(widths))]
    aligned = ret_out.shape[1] % LANES == 0
    local_logs = jnp.sum(log_decay, axis=1)
    log_tile = jnp.broadcast_to(
        jnp.pad(local_logs, (0, -local_logs.shape[0] % 8))[:, None], (-(-local_logs.shape[0] // 8) * 8, LANES)
    )
    projected, logs = project(normed, jnp.concatenate(weights, axis=1), log_tile, n, n_tp)
    logs = logs[:, : local_logs.shape[0], 0]
    sections = jnp.split(projected, points, axis=1)
    tok_count = sections[0].shape[0]
    anchor = lax.axis_index("sp") * tok_count
    positions = anchor + jnp.arange(tok_count, dtype=jnp.int32)
    query_ret = rotate(sections[0].reshape(tok_count, -1, RETAIN_KEY_SIZE), positions).astype(
        jnp.bfloat16
    )
    key_ret = (
        rotate(sections[1].reshape(tok_count, -1, RETAIN_KEY_SIZE), positions)
        * RETAIN_KEY_SIZE ** (-0.5)
    ).astype(jnp.bfloat16)
    value_ret = sections[2].reshape(tok_count, -1, V_DIM)
    stacked = projected[:, points[3] :]
    ret_mix, rim, wholes = retention_path(
        query_ret,
        key_ret,
        value_ret,
        log_decay,
        stacked[tok_count - WINDOW :],
        logs,
        (ret_out, att_out) if aligned else (),
    )
    if not aligned:
        wholes = [
            lax.all_gather(weight, "sp", axis=1, tiled=True)[None] for weight in (ret_out, att_out)
        ]
    att_mix = attention_path(sections[3], stacked, rim, sink_logits, anchor)
    return merge((ret_mix, att_mix), wholes, n_tp)


def solution(mesh):
    in_specs = (
        P(("sp", "tp"), None),
        P(),
        P("sp", "tp"),
        P("sp", "tp"),
        P("sp", "tp"),
        P("tp", "sp"),
        P("sp", "tp"),
        P("sp", "tp"),
        P("sp", "tp"),
        P("tp"),
        P("tp", "sp"),
        P("tp", "sp"),
    )
    out_specs = P(("sp", "tp"), None)
    return jax.shard_map(
        on_device, mesh=mesh, in_specs=in_specs, out_specs=out_specs, check_vma=False
    )
```

profile of v0, /device:TPU:0, one launch (start us, length us, event | category | flops | bytes accessed | tf_op | source)
XLA Modules:
  0.0 167.8 jit_solution(1504293390823768473)
XLA Ops:
  0.0 1.1 fusion.6
  1.1 0.8 reduce_sum.55
  2.0 0.5 fusion.42
  2.7 0.7 reshape.294
  3.4 0.6 reduce_window_sum.24
  4.0 0.2 slice_reduce_fusion
  4.2 0.2 reduce_window_sum.26
  4.4 0.6 copy.79
  5.0 0.7 copy.76
  5.7 0.6 copy.70
  6.3 0.6 copy.80
  6.9 0.6 copy.73
  7.6 0.6 iota_compare_fusion
  8.2 0.8 fusion.20
  9.0 0.9 copy.60
  9.9 0.9 copy.61
  10.8 1.0 multiply_cosine_fusion
  11.8 1.1 fusion.8.normed_ref
  12.9 1.3 concatenate.26.pack_ref
  14.2 71.4 %project_ring.1 = (bf16[256,1664]{1,0:T(8,128)(2,1)S(1)}, f32[8,8,128]{2,1,0:T(8,128)S(1)}) custom-call(bf16[64,2048]{1,0:T(8,128)(2,1)S(1)} %fusion.8.normed_ref, bf16[256,1664]{1,0:T(8,128)(2,1)S(1)} %concatenate.26.pack_ref, f32[8,128]{1,0:T(8,128)S(1)} %broadcast_in_dim.59.log_ref), custom_call_target="tpu_custom_call" | custom-call | flops 429496729600 | bytes 6815744 | tf_op jit(solution)/shard_map/project_ring/pallas_call | solution.py:291
  86.1 0.7 copy.87
  87.2 0.8 copy.64
  88.0 0.8 copy.65
  88.9 0.1 copy.69
  89.1 0.1 copy.68
  89.2 0.1 fusion.13
  89.5 0.3 reshape.305
  89.8 0.3 fusion.22
  90.2 1.7 %while.13 = (s32[]{:T(128)}, f32[2,128,256]{2,1,0:T(8,128)S(1)}, f32[2,2,128,256]{3,2,1,0:T(8,128)}, f32[2,2]{1,0:T(2,128)S(1)}, f32[2,2,128,256]{3,2,1,0:T(8,128)S(1)}, /*index=5*/s32[]{:T(128)}, s32[]{:T(128)}) while((s32[]{:T(128)}, f32[2,128,256]{2,1,0:T(8,128)S(1)}, f32[2,2,128,256]{3,2,1,0:T(8,128)}, f32[2,2]{1,0:T(2,128)S(1)}, ...), condition=%wide.region_4.5_spmd.clone, body=%wide.region_3.4_spmd.clone.sunk | while | flops 262147 | bytes 1310852 | solution.py:70
  90.2 0.7 bitcast_dynamic-update-slice_fusion.2
  91.0 0.7 bitcast_dynamic-update-slice_fusion.2
  92.0 53.7 %state_ring.1 = (bf16[128,128]{1,0:T(8,128)(2,1)S(1)}, bf16[8,2,128,256]{3,2,1,0:T(8,128)(2,1)S(1)}, bf16[8,512,256]{2,1,0:T(8,128)(2,1)S(1)}, bf16[8,512,256]{2,1,0:T(8,128)(2,1)S(1)}) custom-call(bf16[128,128]{1,0:T(8,128)(2,1)S(1)} %slice.47.rim_ref, bf16[2,128,256]{2,1,0:T(8,128)(2,1)S(1)} %convert_element_type.90.state_ref, ...), custom_call_target="tpu_custom_call" | custom-call | flops 21474836480 | bytes 1048576 | tf_op jit(solution)/shard_map/state_ring/pallas_call | solution.py:397
  145.7 1.3 copy-done
  147.0 0.3 multiply_reduce_fusion
  147.4 0.8 fusion.10
  148.1 2.3 %multiply_reduce_fusion.1 = (f32[2,128,2]{1,2,0:T(2,128)S(1)}, f32[2,128,2,256]{1,3,2,0:T(8,128)}) fusion(f32[2,2,256,128]{3,2,1,0:T(8,128)S(1)} %fusion.10, bf16[2,128,2,128]{3,1,2,0:T(8,128)(2,1)} %copy-done.5, f32[2,2,128]{2,0,1:T(2,128)S(1)} %copy-done.13, pred[128,128]{1,0:T(8,128)(4,1)S(1)} %copy-done.12, bf16[2,128,2,64]{3,1,2,0:T(8,128)(2,1)} %copy.65, ...), kind=kOutput, calls=%fused_computation.23 | convolution fusion | flops 51314176 | bytes 1593344 | tf_op jit(solution)/shard_map/hnij,njhv->nihv/dot_general | solution.py:57
  150.4 1.1 multiply_convert_fusion
  151.5 0.2 copy.82
  151.7 0.2 convert_element_type.95
  152.1 0.1 copy.86
  152.2 1.4 fusion.53
  153.7 0.3 fusion.1
  154.1 0.5 fusion.3
  154.6 0.2 reshape.306
  154.8 0.4 copy.105
  155.2 1.6 copy-done.1
  156.8 10.3 %merge_scatter.1 = bf16[64,2048]{1,0:T(8,128)(2,1)S(1)} custom-call(bf16[2,128,512]{2,1,0:T(8,128)(2,1)S(1)} %bitcast.74, bf16[2,128,512]{2,1,0:T(8,128)(2,1)S(1)} %bitcast.73, bf16[8,512,256]{2,1,0:T(8,128)(2,1)S(1)} %get-tuple-element.45.ret_out_ref, bf16[8,512,256]{2,1,0:T(8,128)(2,1)S(1)} %copy-done.1), custom_call_target="tpu_custom_call" | custom-call | flops 1073741824 | bytes 4194304 | tf_op jit(solution)/shard_map/merge_scatter/pallas_call | solution.py:491
  167.1 0.7 copy.129
  (85 shorter events, 2.0 us)
Async XLA Ops:
  0.0 2.7 %copy-start.20 = (pred[8]{0:T(512)(128)(4,1)}, pred[8]{0:T(512)(128)(4,1)S(1)}, u32[]{:S(2)}) copy-start(pred[8]{0:T(512)(128)(4,1)S(1)} %iota_compare_fusion.2) | copy-start | bytes 28
  14.2 71.6 %copy-start.18 = (pred[8,8]{1,0:T(8,128)(4,1)S(1)}, pred[8,8]{1,0:T(8,128)(4,1)}, u32[]{:S(2)}) copy-start(pred[8,8]{1,0:T(8,128)(4,1)} %fusion.42) | copy-start | bytes 196
  14.2 71.6 %copy-start.21 = (pred[8]{0:T(512)(128)(4,1)S(1)}, pred[8]{0:T(512)(128)(4,1)}, u32[]{:S(2)}) copy-start(pred[8]{0:T(512)(128)(4,1)} %copy-done.20) | copy-start | bytes 28
  85.6 1.4 copy-start.10
  85.7 1.4 copy-start.11
  87.2 2.6 %copy-start.15 = (f32[2,128,2]{1,2,0:T(2,128)S(1)}, f32[2,128,2]{1,2,0:T(2,128)}, u32[]{:S(2)}) copy-start(f32[2,128,2]{1,2,0:T(2,128)} %copy.73) | copy-start | bytes 6148
  88.8 1.3 copy-start.4
  88.8 1.3 copy-start.19
  89.4 0.8 copy-start.5
  90.1 1.8 %copy-start.2 = (bf16[512,256]{1,0:T(8,128)(2,1)S(1)}, bf16[512,256]{1,0:T(8,128)(2,1)}, u32[]{:S(2)}) copy-start(bf16[512,256]{1,0:T(8,128)(2,1)} %refs_0_.1) | copy-start | bytes 786436
  90.1 1.8 %copy-start.3 = (bf16[512,256]{1,0:T(8,128)(2,1)S(1)}, bf16[512,256]{1,0:T(8,128)(2,1)}, u32[]{:S(2)}) copy-start(bf16[512,256]{1,0:T(8,128)(2,1)} %refs_1_.1) | copy-start | bytes 786436
  91.9 55.4 %copy-start.6 = (bf16[2,128,2,64]{3,1,2,0:T(8,128)(2,1)S(1)}, bf16[2,128,2,64]{3,1,2,0:T(8,128)(2,1)}, u32[]{:S(2)}) copy-start(bf16[2,128,2,64]{3,1,2,0:T(8,128)(2,1)} %copy.64) | copy-start | bytes 196612
  91.9 55.4 %copy-start.7 = (bf16[2,128,2,64]{3,1,2,0:T(8,128)(2,1)S(1)}, bf16[2,128,2,64]{3,1,2,0:T(8,128)(2,1)}, u32[]{:S(2)}) copy-start(bf16[2,128,2,64]{3,1,2,0:T(8,128)(2,1)} %copy.65) | copy-start | bytes 196612
  91.9 55.4 %copy-start.8 = (f32[2,2,128,256]{3,2,1,0:T(8,128)S(1)}, f32[2,2,128,256]{3,2,1,0:T(8,128)}, u32[]{:S(2)}) copy-start(f32[2,2,128,256]{3,2,1,0:T(8,128)} %get-tuple-element.40) | copy-start | bytes 1572868
  91.9 55.4 %copy-start.14 = (f32[2,128,2]{1,2,0:T(2,128)S(1)}, f32[2,128,2]{1,2,0:T(2,128)}, u32[]{:S(2)}) copy-start(f32[2,128,2]{1,2,0:T(2,128)} %copy.80) | copy-start | bytes 6148
  92.0 55.4 %copy-start.16 = (f32[2,2]{1,0:T(2,128)S(1)}, f32[2,2]{1,0:T(2,128)}, u32[]{:S(2)}) copy-start(f32[2,2]{1,0:T(2,128)} %copy.79) | copy-start | bytes 52
  145.7 1.3 copy-start
  147.0 1.1 copy-start.12
  147.0 1.1 copy-start.13
  151.7 1.9 %copy-start.17 = (f32[8]{0:T(128)S(1)}, f32[8]{0:T(128)}, u32[]{:S(2)}) copy-start(f32[8]{0:T(128)} %param.23) | copy-start | bytes 100
  152.2 1.9 %copy-start.9 = (bf16[2,128,2,1,64]{1,4,0,3,2:T(8,128)(2,1)S(1)}, bf16[2,128,2,1,64]{1,4,0,3,2:T(8,128)(2,1)}, u32[]{:S(2)}) copy-start(bf16[2,128,2,1,64]{1,4,0,3,2:T(8,128)(2,1)} %copy.87) | copy-start | bytes 196612
  155.2 1.6 copy-start.1
where the time goes:
time: 168 us
  Pallas kernels  135 us (80%)
  local copies, waits for them, and re-layouts  15.6 us (9%)
  other arithmetic  10.9 us (6%)
  matrix products  5.28 us (3%)
    pallas_call x1, Pallas kernels, project(): pl.pallas_call(functools.partial(project_kernel, n, n_tp), out_shape=(jax...  71.4 us
    pallas_call x1, Pallas kernels, exchange(): pl.pallas_call(functools.partial(exchange_kernel, n, len(weights)), out_s...  53.7 us
    pallas_call x1, Pallas kernels, merge(): pl.pallas_call(functools.partial(merge_kernel, n_tp), out_shape=jax.Shape...  10.3 us
    unnamed x48, local copies, waits for them, and re-layouts  6.11 us

commit v1 on v0

--- a/solution.py
+++ b/solution.py
@@ -1,4 +1,5 @@
 import functools
+import math
 
 import jax
 import jax.numpy as jnp
@@ -511,6 +512,614 @@
     )(*mixes, *weights)
 
 
+SIDES = 2
+CORES = 2
+
+
+def layer_fits(n, n_tp, shapes):
+    count, heads_here, att_here, kv_here, length = shapes
+    nz, nx = n // SIDES, n_tp // CORES
+    return (
+        n == nz * SIDES
+        and nx == 2
+        and n_tp == nx * CORES
+        and nz == heads_here * CORES
+        and kv_here == 1
+        and att_here * HEAD_DIM == heads_here * V_DIM
+        and count % 16 == 0
+        and n_tp * count == length
+        and length == 2 * WINDOW
+        and length == 2 * BLOCK
+        and nx * WINDOW == length
+    )
+
+
+def layer_scratch(n, n_tp, count, features, depth, width):
+    nz = n // SIDES
+    heads = n_tp * count
+    length = n_tp * count
+    rows = nz * length
+    group = nz * count
+    att_width = V_DIM + 2 * HEAD_DIM
+    ret_width = 2 * RETAIN_KEY_SIZE + V_DIM
+    parts = nz // CORES
+    bf, f32 = jnp.bfloat16, jnp.float32
+    dma = pltpu.SemaphoreType.DMA
+    return dict(
+        tok=pltpu.VMEM((rows, features), bf),
+        ret_pack=pltpu.VMEM((parts, depth, ret_width), bf),
+        att_pack=pltpu.VMEM((parts, depth, att_width), bf),
+        ret_w=pltpu.VMEM((n * depth, ret_width), bf),
+        att_w=pltpu.VMEM((n * depth, att_width), bf),
+        out_w=pltpu.VMEM((n, V_DIM, width), bf),
+        aux=pltpu.VMEM((n, 8, length), f32),
+        cosine=pltpu.VMEM((rows, RETAIN_KEY_SIZE), f32),
+        sine=pltpu.VMEM((rows, RETAIN_KEY_SIZE), f32),
+        fade_q=pltpu.VMEM((rows, RETAIN_KEY_SIZE), f32),
+        fade_k=pltpu.VMEM((rows, RETAIN_KEY_SIZE), f32),
+        decay=pltpu.VMEM((rows, length), f32),
+        queries=pltpu.VMEM((rows, V_DIM), bf),
+        keys=pltpu.VMEM((rows, RETAIN_KEY_SIZE), bf),
+        values=pltpu.VMEM((rows, V_DIM), bf),
+        inner=pltpu.VMEM((rows, V_DIM), f32),
+        states=pltpu.VMEM((nz, SIDES, RETAIN_KEY_SIZE, V_DIM), bf),
+        before=pltpu.VMEM((nz, SIDES, RETAIN_KEY_SIZE, V_DIM), f32),
+        kv=pltpu.VMEM((4, nz, length + WINDOW, 2 * HEAD_DIM), bf),
+        rim=pltpu.VMEM((nz, WINDOW, 2 * HEAD_DIM), bf),
+        halo=pltpu.VMEM((nz, WINDOW, 2 * HEAD_DIM), bf),
+        mix=pltpu.VMEM((rows, V_DIM), bf),
+        core_out=pltpu.VMEM((2, n, group, width), bf),
+        core_in=pltpu.VMEM((2, n, group, width), bf),
+        x_out=pltpu.VMEM((n, group, width), bf),
+        x_in=pltpu.VMEM((n, group, width), bf),
+        acc=pltpu.VMEM((n, group, width), f32),
+        z_out=pltpu.VMEM((n, group, width), bf),
+        z_in=pltpu.VMEM((n, nz, count, width), bf),
+        tz_s=dma((2, nz)),
+        tz_r=dma((nz,)),
+        tx_s=dma((nz,)),
+        tx_r=dma((nz,)),
+        tc_s=dma((nz, 2)),
+        tc_r=dma((nz, 2)),
+        w_s=dma((3, parts, CORES)),
+        w_r=dma((3, nz)),
+        f_s=dma((3, nz)),
+        f_r=dma((3, nz)),
+        s_s=dma((nz,)),
+        s_r=dma((nz,)),
+        h_s=dma((1,)),
+        h_r=dma((1,)),
+        rc_s=dma((2, n)),
+        rc_r=dma((2, n)),
+        rx_s=dma((n,)),
+        rx_r=dma((n,)),
+        rz_s=dma((n, nz)),
+        rz_r=dma((n, nz)),
+    )
+
+
+class Named:
+    def __init__(self, names, refs):
+        for name, ref in zip(names, refs):
+            setattr(self, name, ref)
+
+
+def dot_nt(a, b, **kw):
+    return lax.dot_general(a, b, (((1,), (1,)), ((), ())), preferred_element_type=jnp.float32, **kw)
+
+
+def dot_tn(a, b):
+    return lax.dot_general(a, b, (((0,), (0,)), ((), ())), preferred_element_type=jnp.float32)
+
+
+def dot_nn(a, b):
+    return jnp.dot(a, b, preferred_element_type=jnp.float32)
+
+
+def layer_kernel(n, n_tp, names, *refs):
+    (tokens_ref, gain_ref, aux_ref, rq_ref, rk_ref, rv_ref, aq_ref, ak_ref, av_ref, ro_ref, ao_ref) = refs[:11]
+    out_ref = refs[11]
+    m = Named(names, refs[12:])
+    nz = n // SIDES
+    parts = nz // CORES
+    count, features = tokens_ref.shape
+    depth = rq_ref.shape[0]
+    width = out_ref.shape[1] // n
+    length = n_tp * count
+    group = nz * count
+    key_size = RETAIN_KEY_SIZE
+    bf, f32 = jnp.bfloat16, jnp.float32
+
+    sp, tp = lax.axis_index("sp"), lax.axis_index("tp")
+    z, y = sp // SIDES, lax.rem(sp, SIDES)
+    x, c = tp // CORES, lax.rem(tp, CORES)
+    ny, nx, nc = 1 - y, 1 - x, 1 - c
+    is_ret, is_att = c == 0, c == 1
+    source_core = z // parts
+    part_here = lax.rem(z, parts)
+
+    def device(zz, yy, xx, cc):
+        return (zz * SIDES + yy, xx * CORES + cc)
+
+    def remote(src, dst, send_sem, recv_sem, target):
+        return pltpu.make_async_remote_copy(
+            src_ref=src,
+            dst_ref=dst,
+            send_sem=send_sem,
+            recv_sem=recv_sem,
+            device_id=target,
+            device_id_type=MESH,
+        )
+
+    started = []
+
+    def go(copy, condition=None):
+        started.append((copy, condition))
+        if condition is None:
+            copy.start()
+        else:
+            pl.when(condition)(copy.start)
+
+    def both(*conditions):
+        conditions = [cond for cond in conditions if cond is not None]
+        if not conditions:
+            return None
+        result = conditions[0]
+        for cond in conditions[1:]:
+            result = result & cond
+        return result
+
+    def await_recv(copy, condition=None):
+        if condition is None:
+            copy.wait_recv()
+        else:
+            pl.when(condition)(copy.wait_recv)
+
+    barrier = pltpu.get_barrier_semaphore()
+    peers = [device(z, ny, x, c), device(z, y, nx, c), device(z, y, x, nc)]
+    for step in range(1, nz):
+        for cc in range(CORES):
+            peers.append(device(lax.rem(z + step, nz), y, x, cc))
+    for peer in peers:
+        pl.semaphore_signal(barrier, inc=1, device_id=peer, device_id_type=MESH)
+
+    def token_rows(zz, xx, cc):
+        return pl.ds(pl.multiple_of(zz * length + xx * (CORES * count) + cc * count, count), count)
+
+    tok_float = tokens_ref[...].astype(f32)
+    scale = lax.rsqrt(jnp.mean(tok_float * tok_float, axis=-1, keepdims=True) + epsilon)
+    m.tok[token_rows(z, x, c), :] = (tok_float * scale * gain_ref[...]).astype(bf)
+    for part in range(parts):
+        wide = slice(part * V_DIM, (part + 1) * V_DIM)
+        thin = slice(part * key_size, (part + 1) * key_size)
+        m.ret_pack[part, :, 0:key_size] = rq_ref[:, thin]
+        m.ret_pack[part, :, key_size : 2 * key_size] = rk_ref[:, thin]
+        m.ret_pack[part, :, 2 * key_size :] = rv_ref[:, wide]
+        m.att_pack[part, :, 0:V_DIM] = aq_ref[:, wide]
+        m.att_pack[part, :, V_DIM:] = jnp.concatenate([ak_ref[...], av_ref[...]], axis=1)
+    pl.semaphore_wait(barrier, len(peers))
+
+    def token_at(zz, xx, cc):
+        return m.tok.at[token_rows(zz, xx, cc)]
+
+    def token_z(origin, way):
+        piece = token_at(origin, x, c)
+        return remote(piece, piece, m.tz_s.at[way, origin], m.tz_r.at[origin], device(z + 1 - 2 * way, y, x, c))
+
+    def token_x(origin, side):
+        piece = token_at(origin, side, c)
+        return remote(piece, piece, m.tx_s.at[origin], m.tx_r.at[origin], device(z, y, nx, c))
+
+    def token_core(origin, side, core):
+        piece = token_at(origin, side, core)
+        return remote(piece, piece, m.tc_s.at[origin, side], m.tc_r.at[origin, side], device(z, y, x, nc))
+
+    can_go = (z < nz - 1, z > 0)
+
+    def spread(origin, way, condition):
+        go(token_z(origin, way), both(condition, can_go[way]))
+
+    def weight_rows(zz, yy):
+        return pl.ds(pl.multiple_of((zz * SIDES + yy) * depth, depth), depth)
+
+    def send_weights(part, kind):
+        target_z = c * parts + part
+        for core in range(CORES):
+            other = jnp.logical_not((target_z == z) & (c == core))
+            target = device(target_z, y, x, core)
+            if kind == 0:
+                pack, dest = (m.ret_pack, m.ret_w) if core == 0 else (m.att_pack, m.att_w)
+                src, dst = pack.at[part], dest.at[weight_rows(z, y)]
+            elif kind == 1:
+                held = ro_ref if core == 0 else ao_ref
+                src, dst = held.at[part * V_DIM : (part + 1) * V_DIM], m.out_w.at[sp]
+            else:
+                src, dst = aux_ref, m.aux.at[sp]
+            go(remote(src, dst, m.w_s.at[kind, part, core], m.w_r.at[kind, z], target), other)
+
+            @pl.when(jnp.logical_not(other))
+            def _():
+                if kind == 0:
+                    dest[weight_rows(z, y), :] = pack[part]
+                elif kind == 1:
+                    m.out_w[sp] = held[part * V_DIM : (part + 1) * V_DIM, :]
+                else:
+                    m.aux[sp] = aux_ref[...]
+
+    def weight_piece(kind, zz, yy, core):
+        if kind == 0:
+            return (m.ret_w if core == 0 else m.att_w).at[weight_rows(zz, yy)]
+        if kind == 1:
+            return m.out_w.at[zz * SIDES + yy]
+        return m.aux.at[zz * SIDES + yy]
+
+    def per_core(kind):
+        return ((0, is_ret), (1, is_att)) if kind == 0 else ((0, None),)
+
+    def pass_weights(kind, zz):
+        other = jnp.logical_not((zz == z) & (c == source_core))
+        for core, condition in per_core(kind):
+            piece = weight_piece(kind, zz, y, core)
+            await_recv(
+                remote(piece, piece, m.f_s.at[kind, zz], m.w_r.at[kind, zz], device(z, ny, x, c)),
+                both(condition, other),
+            )
+            go(
+                remote(piece, piece, m.f_s.at[kind, zz], m.f_r.at[kind, zz], device(z, ny, x, c)),
+                condition,
+            )
+
+    def take_weights(kind, zz):
+        for core, condition in per_core(kind):
+            piece = weight_piece(kind, zz, ny, core)
+            await_recv(
+                remote(piece, piece, m.f_s.at[kind, zz], m.f_r.at[kind, zz], device(z, ny, x, c)), condition
+            )
+
+    for part in range(parts):
+        send_weights(part, 2)
+    for way in range(2):
+        spread(z, way, None)
+    go(token_x(z, x))
+    go(token_core(z, x, c))
+    send_weights(0, 0)
+
+    def pass_tokens(step):
+        for way in range(2):
+            origin = z - step if way == 0 else z + step
+            valid = origin >= 0 if way == 0 else origin < nz
+            await_recv(token_z(origin, way), valid)
+            spread(origin, way, valid)
+            go(token_x(origin, x), valid)
+            go(token_core(origin, x, c), valid)
+
+    def around(step):
+        return lax.rem(z + step, nz)
+
+    for step in range(nz):
+        pass_weights(2, around(step))
+    pass_tokens(1)
+    send_weights(1, 0)
+    pass_weights(0, z)
+
+    @pl.when(is_ret)
+    def _():
+        lane = lax.broadcasted_iota(jnp.int32, (length, key_size), 1)
+        row = lax.broadcasted_iota(jnp.int32, (length, key_size), 0)
+        half = key_size // 2
+        inverse = jnp.exp(
+            lax.rem(lane, half).astype(f32) * (-math.log(rope_base) / half)
+        )
+        sign = jnp.where(lane < half, -1.0, 1.0)
+
+        def table(zz, carry):
+            where = pl.ds(pl.multiple_of(zz * length, length), length)
+            angles = (row + (zz * SIDES + y) * length).astype(f32) * inverse
+            m.cosine[where, :] = jnp.cos(angles)
+            m.sine[where, :] = jnp.sin(angles) * sign
+            return carry
+
+        lax.fori_loop(0, nz, table, 0)
+
+    pass_tokens(2)
+    for part in range(parts):
+        send_weights(part, 1)
+    for step in range(1, nz):
+        pass_weights(0, around(step))
+    for step in range(3, nz):
+        pass_tokens(step)
+    for step in range(nz):
+        origin = around(step)
+        await_recv(token_x(origin, nx))
+        go(token_core(origin, nx, c))
+    for zz in range(nz):
+        take_weights(2, zz)
+
+    @pl.when(is_ret)
+    def _():
+        lower = (
+            lax.broadcasted_iota(jnp.int32, (length, length), 0)
+            >= lax.broadcasted_iota(jnp.int32, (length, length), 1)
+        )
+        lower_float = lower.astype(f32)
+        mine = [m.aux[zz * SIDES + y, pl.ds(part_here, 1), :] for zz in range(nz)]
+        logs = jnp.concatenate(mine * (8 // nz), axis=0)
+        by_row = dot_nt(logs, lower_float, precision=lax.Precision.HIGHEST)
+        by_column = dot_nt(lower_float, logs, precision=lax.Precision.HIGHEST)
+        for zz in range(nz):
+            rows = slice(zz * length, (zz + 1) * length)
+            column = by_column[:, zz : zz + 1]
+            closing = by_column[length - 1 : length, zz : zz + 1]
+            within = jnp.minimum(column - by_row[zz : zz + 1, :], 0.0)
+            m.decay[rows, :] = jnp.where(lower, jnp.exp(within), 0.0)
+            m.fade_q[rows, :] = jnp.broadcast_to(jnp.exp(column), (length, key_size))
+            m.fade_k[rows, :] = jnp.broadcast_to(jnp.exp(closing - column), (length, key_size))
+
+    for step in range(nz):
+        take_weights(0, around(step))
+    for step in range(nz):
+        origin = around(step)
+        for side in (x, nx):
+            await_recv(token_core(origin, side, nc))
+
+    def run_rows(zz):
+        return pl.ds(pl.multiple_of(zz * length, length), length)
+
+    def store_mix(zz, xx, lanes, values):
+        for cc in range(CORES):
+            start = ((xx * CORES + cc) * nz + zz) * count
+            m.mix[pl.ds(pl.multiple_of(start, count), count), lanes] = values[cc * count : (cc + 1) * count]
+
+    def state_copy(zz):
+        piece = m.states.at[zz, y]
+        return remote(piece, piece, m.s_s.at[zz], m.s_r.at[zz], device(z, ny, x, c))
+
+    def state_arrival(zz):
+        piece = m.states.at[zz, ny]
+        return remote(piece, piece, m.s_s.at[zz], m.s_r.at[zz], device(z, ny, x, c))
+
+    halo_copy = remote(m.rim, m.halo, m.h_s.at[0], m.h_r.at[0], device(z, ny, x, c))
+
+    @pl.when(is_ret)
+    def _():
+        def project_run(zz, carry):
+            rows = run_rows(zz)
+            product = dot_nn(m.tok[rows, :], m.ret_w[...]).astype(bf)
+            cosine, sine = m.cosine[rows, :], m.sine[rows, :]
+
+            def turn(values):
+                values = values.astype(f32)
+                return values * cosine + pltpu.roll(values, key_size // 2, 1) * sine
+
+            m.queries[rows, 0:key_size] = turn(product[:, 0:key_size]).astype(bf)
+            key = (turn(product[:, key_size : 2 * key_size]) * key_size ** (-0.5)).astype(bf)
+            m.keys[rows, :] = key
+            value = product[:, 2 * key_size :]
+            m.values[rows, :] = value
+            faded = (key.astype(f32) * m.fade_k[rows, :]).astype(bf)
+            m.states[zz, y] = dot_tn(faded, value).astype(bf)
+            state_copy(zz).start()
+            return carry
+
+        lax.fori_loop(0, nz, project_run, 0)
+
+    lane_kv = lax.broadcasted_iota(jnp.int32, (WINDOW, 2 * HEAD_DIM), 1)
+
+    def place(zz, spot, packed):
+        where = pl.ds(spot * WINDOW, WINDOW)
+        packed = packed.astype(f32)
+        low = jnp.where(lane_kv < HEAD_DIM, packed, 0.0)
+        high = jnp.where(lane_kv < HEAD_DIM, 0.0, packed)
+        m.kv[0, zz, where, :] = low.astype(bf)
+        m.kv[1, zz, where, :] = pltpu.roll(low, HEAD_DIM, 1).astype(bf)
+        m.kv[2, zz, where, :] = pltpu.roll(high, HEAD_DIM, 1).astype(bf)
+        m.kv[3, zz, where, :] = high.astype(bf)
+
+    @pl.when(is_att)
+    def _():
+        def project_run(zz, carry):
+            rows = run_rows(zz)
+            product = dot_nn(m.tok[rows, :], m.att_w[...]).astype(bf)
+            m.queries[rows, :] = product[:, 0:V_DIM]
+            for spot in range(2):
+                place(zz, spot + 1, product[spot * WINDOW : (spot + 1) * WINDOW, V_DIM:])
+            m.rim[zz] = product[length - WINDOW :, V_DIM:]
+            return carry
+
+        lax.fori_loop(0, nz, project_run, 0)
+        halo_copy.start()
+
+    for step in range(nz):
+        pass_weights(1, around(step))
+
+    @pl.when(is_ret)
+    def _():
+        def inner_run(zz, carry):
+            rows = run_rows(zz)
+            scores = dot_nt(m.queries[rows, 0:key_size], m.keys[rows, :]) * m.decay[rows, :]
+            m.inner[rows, :] = dot_nn(scores.astype(bf), m.values[rows, :])
+            return carry
+
+        lax.fori_loop(0, nz, inner_run, 0)
+        totals = [
+            jnp.sum(m.aux[spot, pl.ds(part_here, 1), :], axis=1, keepdims=True) for spot in range(n)
+        ]
+        for zz in range(nz):
+            state_arrival(zz).wait_recv()
+        running = jnp.zeros((key_size, V_DIM), f32)
+        for zz in range(nz):
+            for yy in range(SIDES):
+                m.before[zz, yy] = running
+                running = running * jnp.exp(totals[zz * SIDES + yy]) + m.states[zz, yy].astype(f32)
+
+        def finish_run(zz, carry):
+            rows = run_rows(zz)
+            query = (m.queries[rows, 0:key_size].astype(f32) * m.fade_q[rows, :]).astype(bf)
+            state = m.before[zz, y]
+            high = state.astype(bf)
+            low = (state - high.astype(f32)).astype(bf)
+            total = m.inner[rows, :] + (dot_nn(query, high) + dot_nn(query, low))
+            total = total * lax.rsqrt(jnp.mean(total * total, axis=-1, keepdims=True) + epsilon)
+            total = total.astype(bf)
+            for xx in range(2):
+                store_mix(zz, xx, slice(0, V_DIM), total[xx * WINDOW : (xx + 1) * WINDOW])
+            return carry
+
+        lax.fori_loop(0, nz, finish_run, 0)
+        for zz in range(nz):
+            state_copy(zz).wait_send()
+
+    @pl.when(is_att)
+    def _():
+        halo_copy.wait_recv()
+        for zz in range(nz):
+            place(zz, 0, m.halo[jnp.maximum(zz - 1 + y, 0)])
+        row = lax.broadcasted_iota(jnp.int32, (WINDOW, 2 * WINDOW), 0)
+        column = lax.broadcasted_iota(jnp.int32, (WINDOW, 2 * WINDOW), 1)
+        band = (column > row) & (column <= row + WINDOW)
+        sink_row = m.aux[sp, parts : parts + 1, 0:LANES]
+        sink_lane = lax.broadcasted_iota(jnp.int32, (1, LANES), 1)
+        heads = V_DIM // HEAD_DIM
+        sinks = [
+            jnp.sum(
+                jnp.where(sink_lane == part_here * heads + head, sink_row, 0.0), axis=1, keepdims=True
+            )
+            for head in range(heads)
+        ]
+
+        def attend_run(zz, carry):
+            for xx in range(2):
+                first = (zz + y + xx) == 0
+                allowed = band & ((column >= WINDOW) | jnp.logical_not(first))
+                where = pl.ds(xx * WINDOW, 2 * WINDOW)
+                rows = pl.ds(pl.multiple_of(zz * length + xx * WINDOW, WINDOW), WINDOW)
+                for pair in range(heads // 2):
+                    lanes = slice(pair * LANES, (pair + 1) * LANES)
+                    query = m.queries[rows, lanes]
+                    mixed = None
+                    for side in range(2):
+                        sink = sinks[pair * 2 + side]
+                        scores = dot_nt(query, m.kv[side, zz, where, :]) * HEAD_DIM ** (-0.5)
+                        scores = jnp.where(allowed, scores, masked_out)
+                        highest = jnp.maximum(jnp.max(scores, axis=-1, keepdims=True), sink)
+                        lifted = jnp.exp(scores - highest)
+                        below = jnp.sum(lifted, axis=-1, keepdims=True) + jnp.exp(sink - highest)
+                        weights = (lifted / below).astype(bf)
+                        term = dot_nn(weights, m.kv[2 + side, zz, where, :])
+                        mixed = term if mixed is None else mixed + term
+                    store_mix(zz, xx, lanes, mixed.astype(bf))
+            return carry
+
+        lax.fori_loop(0, nz, attend_run, 0)
+        halo_copy.wait_send()
+
+    for step in range(nz):
+        take_weights(1, around(step))
+
+    def mix_rows(xx, cc):
+        return pl.ds(pl.multiple_of((xx * CORES + cc) * group, group), group)
+
+    def core_copy(slot, q):
+        return remote(
+            m.core_out.at[slot, q], m.core_in.at[slot, q], m.rc_s.at[slot, q], m.rc_r.at[slot, q],
+            device(z, y, x, nc),
+        )
+
+    def x_copy(q):
+        return remote(m.x_out.at[q], m.x_in.at[q], m.rx_s.at[q], m.rx_r.at[q], device(z, y, nx, c))
+
+    def home_rows(zz):
+        return pl.ds(pl.multiple_of(zz * count, count), count)
+
+    def z_copy(q, zz):
+        return remote(
+            m.z_out.at[q, home_rows(zz)], m.z_in.at[q, z], m.rz_s.at[q, zz], m.rz_r.at[q, z],
+            device(zz, y, x, c),
+        )
+
+    def z_arrival(q, zz):
+        return remote(
+            m.z_out.at[q, home_rows(zz)], m.z_in.at[q, zz], m.rz_s.at[q, zz], m.rz_r.at[q, zz],
+            device(zz, y, x, c),
+        )
+
+    def to_core(slot, xx):
+        def body(q, carry):
+            m.core_out[slot, q] = dot_nn(m.mix[mix_rows(xx, nc), :], m.out_w[q]).astype(bf)
+            core_copy(slot, q).start()
+            return carry
+
+        lax.fori_loop(0, n, body, 0)
+
+    to_core(0, nx)
+
+    def to_x(q, carry):
+        own = dot_nn(m.mix[mix_rows(nx, c), :], m.out_w[q])
+        core_copy(0, q).wait_recv()
+        m.x_out[q] = (own + m.core_in[0, q].astype(f32)).astype(bf)
+        x_copy(q).start()
+        return carry
+
+    lax.fori_loop(0, n, to_x, 0)
+    to_core(1, x)
+
+    def to_z(q, carry):
+        own = dot_nn(m.mix[mix_rows(x, c), :], m.out_w[q])
+        core_copy(1, q).wait_recv()
+        own = own + m.core_in[1, q].astype(f32)
+        x_copy(q).wait_recv()
+        own = own + m.x_in[q].astype(f32)
+        m.acc[q] = own
+        m.z_out[q] = own.astype(bf)
+        for step in range(1, nz):
+            z_copy(q, around(step)).start()
+        return carry
+
+    lax.fori_loop(0, n, to_z, 0)
+    for q in range(n):
+        total = m.acc[q, home_rows(z), :]
+        for step in range(1, nz):
+            z_arrival(q, around(step)).wait_recv()
+            total = total + m.z_in[q, around(step)].astype(f32)
+        out_ref[:, q * width : (q + 1) * width] = total.astype(bf)
+
+    for copy, condition in started:
+        if condition is None:
+            copy.wait_send()
+        else:
+            pl.when(condition)(copy.wait_send)
+
+    def drain(q, carry):
+        for slot in range(2):
+            core_copy(slot, q).wait_send()
+        x_copy(q).wait_send()
+        for step in range(1, nz):
+            z_copy(q, around(step)).wait_send()
+        return carry
+
+    lax.fori_loop(0, n, drain, 0)
+
+
+def layer(n, n_tp, tokens, norm_gain, aux, *weights):
+    count, features = tokens.shape
+    depth = weights[0].shape[0]
+    width = weights[-1].shape[1]
+    scratch = layer_scratch(n, n_tp, count, features, depth, width)
+    vmem = pl.BlockSpec(memory_space=pltpu.VMEM)
+    return pl.pallas_call(
+        functools.partial(layer_kernel, n, n_tp, tuple(scratch)),
+        out_shape=jax.ShapeDtypeStruct((count, n * width), jnp.bfloat16),
+        in_specs=[vmem] * (3 + len(weights)),
+        out_specs=vmem,
+        scratch_shapes=list(scratch.values()),
+        compiler_params=pltpu.CompilerParams(
+            collective_id=3, has_side_effects=True, vmem_limit_bytes=60 * 2**20
+        ),
+        cost_estimate=pl.CostEstimate(flops=4 * 2**30, bytes_accessed=16 * 2**20, transcendentals=0),
+        name="layer",
+    )(tokens, norm_gain.reshape(1, -1), aux, *weights)
+
+
 def on_device(
     tokens,
     norm_gain,
@@ -525,13 +1134,29 @@
     ret_out,
     att_out,
 ):
+    n, n_tp = lax.axis_size("sp"), lax.axis_size("tp")
+    length = log_decay.shape[1]
+    shapes = (
+        tokens.shape[0],
+        log_decay.shape[0],
+        sink_logits.shape[0],
+        att_key.shape[1] // HEAD_DIM,
+        length,
+    )
+    if layer_fits(n, n_tp, shapes):
+        aux = jnp.concatenate(
+            [log_decay, jnp.pad(sink_logits[None], ((0, 7 - log_decay.shape[0]), (0, length - sink_logits.shape[0])))], axis=0
+        )
+        return layer(
+            n, n_tp, tokens, norm_gain, aux,
+            ret_query, ret_key, ret_value, att_query, att_key, att_value, ret_out, att_out,
+        )
     tok_float = tokens.astype(jnp.float32)
     normed = (
         tok_float
         * lax.rsqrt(jnp.mean(tok_float * tok_float, axis=-1, keepdims=True) + epsilon)
         * norm_gain
     ).astype(jnp.bfloat16)
-    n, n_tp = lax.axis_size("sp"), lax.axis_size("tp")
     weights = (ret_query, ret_key, ret_value, att_query, att_key, att_value)
     widths = [weight.shape[1] for weight in weights]
     points = [sum(widths[:index]) for index in range(1, len(widths))]

time: 168 us -> 117 us (0.70)
  Pallas kernels: 135 us -> 112 us
  local copies, waits for them, and re-layouts: 15.6 us -> 4.59 us
  other arithmetic: 10.9 us -> 0.6 us
  matrix products: 5.28 us -> 0 us
    pallas_call x3 -> x1, Pallas kernels: 135 us -> 112 us  [layer(): pl.pallas_call(functools.partial(layer_kernel, n, n_tp, tuple(scratch)),...]
    dot_general x5 -> x0, matrix products: 5.28 us -> none  [the longest x1 2.28 us: retention_path(): jnp.einsum('hnij,njhv->nihv', scores.astype(jnp.bfloat16), v_blocks, pref...]
    concatenate x9 -> x0, local copies, waits for them, and re-layouts: 3.33 us -> none  [the longest x8 2 us: rotate(): jnp.concatenate([first_half * cosine - second_half * sine_part, second_ha...]
    reduce_sum x5 -> x0, other arithmetic: 2.58 us -> none  [the longest x1 1.1 us: on_device(): jnp.mean(tok_float * tok_float, axis=-1, keepdims=True) + epsilon]
    convert_element_type x5 -> x0, other arithmetic: 2.33 us -> none  [the longest x1 1.09 us: retention_path(): final_product.reshape(tok_count, heads_here * V_DIM).astype(jnp.bfloat16)]
    unnamed x48 -> x9, local copies, waits for them, and re-layouts: 6.11 us -> 4.59 us
where the time goes in v1:
time: 117 us
  Pallas kernels  112 us (96%)
  local copies, waits for them, and re-layouts  4.59 us (4%)
    pallas_call x1, Pallas kernels, layer(): pl.pallas_call(functools.partial(layer_kernel, n, n_tp, tuple(scratch)),...  112 us
    unnamed x9, local copies, waits for them, and re-layouts  4.59 us

profile of v1, /device:TPU:0, one launch (start us, length us, event | category | flops | bytes accessed | tf_op | source)
XLA Modules:
  0.0 116.8 jit_solution(16769334017963348945)
XLA Ops:
  0.0 0.0 copy-start.1
  0.0 0.0 copy-start.2
  0.0 0.7 copy-done.1
  0.7 0.0 copy-done.2
  0.7 0.6 select_maximum_fusion.refs_2_
  1.3 0.0 copy-start
  1.3 1.5 %copy.13.refs_7_ = bf16[256,64]{1,0:T(8,128)(2,1)} copy(bf16[256,64]{0,1:T(8,128)(2,1)} %param.19) | data formatting | bytes 65536 | tf_op args[7]
  2.8 0.0 copy-done
  2.8 0.7 copy.14.refs_8_
  3.5 111.6 %layer.1 = bf16[64,2048]{1,0:T(8,128)(2,1)} custom-call(bf16[64,2048]{1,0:T(8,128)(2,1)} %refs_0_.1, f32[1,2048]{1,0:T(1,128)} %bitcast.3, f32[8,256]{1,0:T(8,128)} %select_maximum_fusion.refs_2_, bf16[256,256]{1,0:T(8,128)(2,1)} %refs_3_.1, bf16[256,256]{1,0:T(8,128)(2,1)} %refs_4_.1, bf16[256,512]{1,0:T(8,128)(2,1)} %refs_5_.1, bf16[256,512]{1,0:T(8,128)(2,1)} %refs_6_.1, ...), custom_call_target="tpu_custom_call" | custom-call | flops 4294967296 | bytes 16777216 | tf_op jit(solution)/shard_map/layer/pallas_call | solution.py:1109
  115.1 1.7 %copy.16 = bf16[64,2048]{1,0:T(8,128)(2,1)} copy(bf16[64,2048]{1,0:T(8,128)(2,1)} %layer.1) | data formatting | bytes 524288
Async XLA Ops:
  0.0 0.7 copy-start.1
  0.0 0.7 copy-start.2
  1.3 1.5 %copy-start = (bf16[256,64]{0,1:T(8,128)(2,1)S(1)}, bf16[256,64]{0,1:T(8,128)(2,1)}, u32[]{:S(2)}) copy-start(bf16[256,64]{0,1:T(8,128)(2,1)} %param.20) | copy-start | bytes 98308

commit v2 on v1

--- a/solution.py
+++ b/solution.py
@@ -514,6 +514,8 @@
 
 SIDES = 2
 CORES = 2
+PAIR = 2
+PIECES = 2
 
 
 def layer_fits(n, n_tp, shapes):
@@ -523,6 +525,7 @@
         n == nz * SIDES
         and nx == 2
         and n_tp == nx * CORES
+        and nz == 2 * PAIR
         and nz == heads_here * CORES
         and kv_here == 1
         and att_here * HEAD_DIM == heads_here * V_DIM
@@ -536,10 +539,9 @@
 
 def layer_scratch(n, n_tp, count, features, depth, width):
     nz = n // SIDES
-    heads = n_tp * count
     length = n_tp * count
     rows = nz * length
-    group = nz * count
+    slab = n * width // PIECES
     att_width = V_DIM + 2 * HEAD_DIM
     ret_width = 2 * RETAIN_KEY_SIZE + V_DIM
     parts = nz // CORES
@@ -551,7 +553,13 @@
         att_pack=pltpu.VMEM((parts, depth, att_width), bf),
         ret_w=pltpu.VMEM((n * depth, ret_width), bf),
         att_w=pltpu.VMEM((n * depth, att_width), bf),
-        out_w=pltpu.VMEM((n, V_DIM, width), bf),
+        out_pack=pltpu.VMEM((2, parts * V_DIM, width), bf),
+        out_w=pltpu.VMEM((V_DIM, n * width), bf),
+        tokens=pltpu.VMEM((count, features), bf),
+        gain=pltpu.VMEM((1, features), f32),
+        aux_here=pltpu.VMEM((8, length), f32),
+        kv_pack=pltpu.VMEM((2 * HEAD_DIM, depth), bf),
+        bias=pltpu.VMEM((2, WINDOW, 2 * WINDOW), f32),
         aux=pltpu.VMEM((n, 8, length), f32),
         cosine=pltpu.VMEM((rows, RETAIN_KEY_SIZE), f32),
         sine=pltpu.VMEM((rows, RETAIN_KEY_SIZE), f32),
@@ -567,21 +575,22 @@
         kv=pltpu.VMEM((4, nz, length + WINDOW, 2 * HEAD_DIM), bf),
         rim=pltpu.VMEM((nz, WINDOW, 2 * HEAD_DIM), bf),
         halo=pltpu.VMEM((nz, WINDOW, 2 * HEAD_DIM), bf),
-        mix=pltpu.VMEM((rows, V_DIM), bf),
-        core_out=pltpu.VMEM((2, n, group, width), bf),
-        core_in=pltpu.VMEM((2, n, group, width), bf),
-        x_out=pltpu.VMEM((n, group, width), bf),
-        x_in=pltpu.VMEM((n, group, width), bf),
-        acc=pltpu.VMEM((n, group, width), f32),
-        z_out=pltpu.VMEM((n, group, width), bf),
-        z_in=pltpu.VMEM((n, nz, count, width), bf),
+        mix=pltpu.VMEM((length, V_DIM), bf),
+        part=pltpu.VMEM((length, slab), f32),
+        keep=pltpu.VMEM((2, nz, PIECES, count, slab), f32),
+        core_out=pltpu.VMEM((2, nz, PIECES, count, slab), bf),
+        core_in=pltpu.VMEM((2, nz, PIECES, count, slab), bf),
+        x_out=pltpu.VMEM((nz, PIECES, count, slab), bf),
+        x_in=pltpu.VMEM((nz, PIECES, count, slab), bf),
+        z_out=pltpu.VMEM((nz, PIECES, count, slab), bf),
+        z_in=pltpu.VMEM((nz, PIECES, count, slab), bf),
         tz_s=dma((2, nz)),
         tz_r=dma((nz,)),
         tx_s=dma((nz,)),
         tx_r=dma((nz,)),
         tc_s=dma((nz, 2)),
         tc_r=dma((nz, 2)),
-        w_s=dma((3, parts, CORES)),
+        w_s=dma((3, nz, CORES)),
         w_r=dma((3, nz)),
         f_s=dma((3, nz)),
         f_r=dma((3, nz)),
@@ -589,12 +598,13 @@
         s_r=dma((nz,)),
         h_s=dma((1,)),
         h_r=dma((1,)),
-        rc_s=dma((2, n)),
-        rc_r=dma((2, n)),
-        rx_s=dma((n,)),
-        rx_r=dma((n,)),
-        rz_s=dma((n, nz)),
-        rz_r=dma((n, nz)),
+        rc_s=dma((2, nz, PIECES)),
+        rc_r=dma((2, nz, PIECES)),
+        rx_s=dma((nz, PIECES)),
+        rx_r=dma((nz, PIECES)),
+        rz_s=dma((nz, PIECES)),
+        rz_r=dma((nz, PIECES)),
+        load=dma((16,)),
     )
 
 
@@ -626,7 +636,7 @@
     depth = rq_ref.shape[0]
     width = out_ref.shape[1] // n
     length = n_tp * count
-    group = nz * count
+    slab = out_ref.shape[1] // PIECES
     key_size = RETAIN_KEY_SIZE
     bf, f32 = jnp.bfloat16, jnp.float32
 
@@ -636,6 +646,7 @@
     ny, nx, nc = 1 - y, 1 - x, 1 - c
     is_ret, is_att = c == 0, c == 1
     source_core = z // parts
+    mate = z + 1 - 2 * lax.rem(z, PAIR)
     part_here = lax.rem(z, parts)
 
     def device(zz, yy, xx, cc):
@@ -675,6 +686,23 @@
         else:
             pl.when(condition)(copy.wait_recv)
 
+    moves = [(tokens_ref, m.tokens), (gain_ref, m.gain), (aux_ref, m.aux_here)]
+    moves += [(ak_ref, m.kv_pack.at[0:HEAD_DIM]), (av_ref, m.kv_pack.at[HEAD_DIM:])]
+    for part in range(parts):
+        wide = slice(part * V_DIM, (part + 1) * V_DIM)
+        thin = slice(part * key_size, (part + 1) * key_size)
+        moves += [
+            (rq_ref.at[:, thin], m.ret_pack.at[part, :, 0:key_size]),
+            (rk_ref.at[:, thin], m.ret_pack.at[part, :, key_size : 2 * key_size]),
+            (rv_ref.at[:, wide], m.ret_pack.at[part, :, 2 * key_size :]),
+            (aq_ref.at[:, wide], m.att_pack.at[part, :, 0:V_DIM]),
+        ]
+    moves += [(ro_ref, m.out_pack.at[0]), (ao_ref, m.out_pack.at[1])]
+    loads = []
+    for index, (src, dst) in enumerate(moves):
+        loads.append(pltpu.make_async_copy(src, dst, m.load.at[index]))
+        loads[-1].start()
+
     barrier = pltpu.get_barrier_semaphore()
     peers = [device(z, ny, x, c), device(z, y, nx, c), device(z, y, x, nc)]
     for step in range(1, nz):
@@ -686,17 +714,16 @@
     def token_rows(zz, xx, cc):
         return pl.ds(pl.multiple_of(zz * length + xx * (CORES * count) + cc * count, count), count)
 
-    tok_float = tokens_ref[...].astype(f32)
+    loads[0].wait()
+    loads[1].wait()
+    tok_float = m.tokens[...].astype(f32)
     scale = lax.rsqrt(jnp.mean(tok_float * tok_float, axis=-1, keepdims=True) + epsilon)
-    m.tok[token_rows(z, x, c), :] = (tok_float * scale * gain_ref[...]).astype(bf)
+    m.tok[token_rows(z, x, c), :] = (tok_float * scale * m.gain[...]).astype(bf)
+    for copy in loads[2:]:
+        copy.wait()
+    pair = jnp.transpose(m.kv_pack[...].astype(f32)).astype(bf)
     for part in range(parts):
-        wide = slice(part * V_DIM, (part + 1) * V_DIM)
-        thin = slice(part * key_size, (part + 1) * key_size)
-        m.ret_pack[part, :, 0:key_size] = rq_ref[:, thin]
-        m.ret_pack[part, :, key_size : 2 * key_size] = rk_ref[:, thin]
-        m.ret_pack[part, :, 2 * key_size :] = rv_ref[:, wide]
-        m.att_pack[part, :, 0:V_DIM] = aq_ref[:, wide]
-        m.att_pack[part, :, V_DIM:] = jnp.concatenate([ak_ref[...], av_ref[...]], axis=1)
+        m.att_pack[part, :, V_DIM:] = pair
     pl.semaphore_wait(barrier, len(peers))
 
     def token_at(zz, xx, cc):
@@ -722,41 +749,62 @@
     def weight_rows(zz, yy):
         return pl.ds(pl.multiple_of((zz * SIDES + yy) * depth, depth), depth)
 
-    def send_weights(part, kind):
-        target_z = c * parts + part
+    near, distant = c == z // parts, c != z // parts
+
+    def toward(step):
+        return (z, mate, lax.rem(z + PAIR, nz), nz - 1 - z)[step]
+
+    def send_weights(step, kind):
+        target_z = toward(step)
+        part = lax.rem(target_z, parts)
+        valid = near if step < PAIR else distant
+        first = len(started)
         for core in range(CORES):
-            other = jnp.logical_not((target_z == z) & (c == core))
             target = device(target_z, y, x, core)
+            pack, dest = (m.ret_pack, m.ret_w) if core == 0 else (m.att_pack, m.att_w)
+            rows = pl.ds(pl.multiple_of(part * V_DIM, V_DIM), V_DIM)
             if kind == 0:
-                pack, dest = (m.ret_pack, m.ret_w) if core == 0 else (m.att_pack, m.att_w)
-                src, dst = pack.at[part], dest.at[weight_rows(z, y)]
+                src = pack.at[part]
             elif kind == 1:
-                held = ro_ref if core == 0 else ao_ref
-                src, dst = held.at[part * V_DIM : (part + 1) * V_DIM], m.out_w.at[sp]
+                src = m.out_pack.at[core, rows]
             else:
-                src, dst = aux_ref, m.aux.at[sp]
-            go(remote(src, dst, m.w_s.at[kind, part, core], m.w_r.at[kind, z], target), other)
-
-            @pl.when(jnp.logical_not(other))
-            def _():
-                if kind == 0:
-                    dest[weight_rows(z, y), :] = pack[part]
-                elif kind == 1:
-                    m.out_w[sp] = held[part * V_DIM : (part + 1) * V_DIM, :]
-                else:
-                    m.aux[sp] = aux_ref[...]
+                src = m.aux_here
+            dst = weight_piece(kind, z, y, core)
+            away = valid if step else valid & (c != core)
+            go(remote(src, dst, m.w_s.at[kind, step, core], m.w_r.at[kind, z], target), away)
+            if step == 0:
+
+                @pl.when(valid & (c == core))
+                def _():
+                    if kind == 0:
+                        dest[weight_rows(z, y), :] = pack[part]
+                    elif kind == 1:
+                        m.out_w[:, out_columns(z, y)] = m.out_pack[core, rows, :]
+                    else:
+                        m.aux[sp] = m.aux_here[...]
+
+        return started[first:]
+
+    def finish(copies):
+        for entry in copies:
+            started[:] = [kept for kept in started if kept is not entry]
+            pl.when(entry[1])(entry[0].wait_send)
+
+    def out_columns(zz, yy):
+        return pl.ds(pl.multiple_of((zz * SIDES + yy) * width, width), width)
 
     def weight_piece(kind, zz, yy, core):
         if kind == 0:
             return (m.ret_w if core == 0 else m.att_w).at[weight_rows(zz, yy)]
         if kind == 1:
-            return m.out_w.at[zz * SIDES + yy]
+            return m.out_w.at[:, out_columns(zz, yy)]
         return m.aux.at[zz * SIDES + yy]
 
     def per_core(kind):
         return ((0, is_ret), (1, is_att)) if kind == 0 else ((0, None),)
 
-    def pass_weights(kind, zz):
+    def pass_weights(kind, step):
+        zz = toward(step)
         other = jnp.logical_not((zz == z) & (c == source_core))
         for core, condition in per_core(kind):
             piece = weight_piece(kind, zz, y, core)
@@ -776,13 +824,15 @@
                 remote(piece, piece, m.f_s.at[kind, zz], m.f_r.at[kind, zz], device(z, ny, x, c)), condition
             )
 
-    for part in range(parts):
-        send_weights(part, 2)
+    for step in range(nz):
+        send_weights(step, 2)
     for way in range(2):
         spread(z, way, None)
     go(token_x(z, x))
     go(token_core(z, x, c))
-    send_weights(0, 0)
+    for kind in range(2):
+        for step in range(PAIR):
+            send_weights(step, kind)
 
     def pass_tokens(step):
         for way in range(2):
@@ -793,14 +843,10 @@
             go(token_x(origin, x), valid)
             go(token_core(origin, x, c), valid)
 
-    def around(step):
-        return lax.rem(z + step, nz)
-
-    for step in range(nz):
-        pass_weights(2, around(step))
-    pass_tokens(1)
-    send_weights(1, 0)
-    pass_weights(0, z)
+    def across_tokens(step):
+        origin = toward(step)
+        await_recv(token_x(origin, nx))
+        go(token_core(origin, nx, c))
 
     @pl.when(is_ret)
     def _():
@@ -821,17 +867,27 @@
 
         lax.fori_loop(0, nz, table, 0)
 
+    pass_weights(0, 0)
+    pass_tokens(1)
+    second = send_weights(2, 0)
+    for step in range(nz):
+        pass_weights(2, step)
+    pass_weights(0, 1)
+    pass_weights(1, 0)
     pass_tokens(2)
-    for part in range(parts):
-        send_weights(part, 1)
-    for step in range(1, nz):
-        pass_weights(0, around(step))
-    for step in range(3, nz):
-        pass_tokens(step)
-    for step in range(nz):
-        origin = around(step)
-        await_recv(token_x(origin, nx))
-        go(token_core(origin, nx, c))
+    across_tokens(0)
+    pass_weights(1, 1)
+    finish(second)
+    third = send_weights(3, 0)
+    pass_tokens(3)
+    pass_weights(0, 2)
+    across_tokens(1)
+    finish(third)
+    send_weights(2, 1)
+    send_weights(3, 1)
+    pass_weights(0, 3)
+    across_tokens(3)
+    across_tokens(2)
     for zz in range(nz):
         take_weights(2, zz)
 
@@ -856,19 +912,14 @@
             m.fade_k[rows, :] = jnp.broadcast_to(jnp.exp(closing - column), (length, key_size))
 
     for step in range(nz):
-        take_weights(0, around(step))
+        take_weights(0, toward(step))
     for step in range(nz):
-        origin = around(step)
+        origin = toward(step)
         for side in (x, nx):
             await_recv(token_core(origin, side, nc))
 
     def run_rows(zz):
         return pl.ds(pl.multiple_of(zz * length, length), length)
-
-    def store_mix(zz, xx, lanes, values):
-        for cc in range(CORES):
-            start = ((xx * CORES + cc) * nz + zz) * count
-            m.mix[pl.ds(pl.multiple_of(start, count), count), lanes] = values[cc * count : (cc + 1) * count]
 
     def state_copy(zz):
         piece = m.states.at[zz, y]
@@ -909,18 +960,18 @@
         where = pl.ds(spot * WINDOW, WINDOW)
         packed = packed.astype(f32)
         low = jnp.where(lane_kv < HEAD_DIM, packed, 0.0)
-        high = jnp.where(lane_kv < HEAD_DIM, 0.0, packed)
+        turned = pltpu.roll(packed, HEAD_DIM, 1)
         m.kv[0, zz, where, :] = low.astype(bf)
         m.kv[1, zz, where, :] = pltpu.roll(low, HEAD_DIM, 1).astype(bf)
-        m.kv[2, zz, where, :] = pltpu.roll(high, HEAD_DIM, 1).astype(bf)
-        m.kv[3, zz, where, :] = high.astype(bf)
+        m.kv[2, zz, where, :] = jnp.where(lane_kv < HEAD_DIM, turned, 1.0).astype(bf)
+        m.kv[3, zz, where, :] = jnp.where(lane_kv < HEAD_DIM, 1.0, packed).astype(bf)
 
     @pl.when(is_att)
     def _():
         def project_run(zz, carry):
             rows = run_rows(zz)
             product = dot_nn(m.tok[rows, :], m.att_w[...]).astype(bf)
-            m.queries[rows, :] = product[:, 0:V_DIM]
+            m.queries[rows, :] = (product[:, 0:V_DIM].astype(f32) * HEAD_DIM ** (-0.5)).astype(bf)
             for spot in range(2):
                 place(zz, spot + 1, product[spot * WINDOW : (spot + 1) * WINDOW, V_DIM:])
             m.rim[zz] = product[length - WINDOW :, V_DIM:]
@@ -929,8 +980,67 @@
         lax.fori_loop(0, nz, project_run, 0)
         halo_copy.start()
 
-    for step in range(nz):
-        pass_weights(1, around(step))
+    far = jnp.where(z < PAIR, nz - 1, 0)
+
+    def home(turn):
+        near = far + jnp.where(z < PAIR, -1, 1)
+        if isinstance(turn, int):
+            return (far, near, mate, z)[turn]
+        return jnp.where(turn == 0, far, jnp.where(turn == 1, near, jnp.where(turn == 2, mate, z)))
+
+    def core_copy(slot, turn, piece):
+        return remote(
+            m.core_out.at[slot, turn, piece],
+            m.core_in.at[slot, turn, piece],
+            m.rc_s.at[slot, turn, piece],
+            m.rc_r.at[slot, turn, piece],
+            device(z, y, x, nc),
+        )
+
+    def x_copy(turn, piece):
+        return remote(
+            m.x_out.at[turn, piece],
+            m.x_in.at[turn, piece],
+            m.rx_s.at[turn, piece],
+            m.rx_r.at[turn, piece],
+            device(z, y, nx, c),
+        )
+
+    def z_copy(turn, piece, target_z, slot):
+        return remote(
+            m.z_out.at[turn, piece],
+            m.z_in.at[slot, piece],
+            m.rz_s.at[turn, piece],
+            m.rz_r.at[slot, piece],
+            device(target_z, y, x, c),
+        )
+
+    def take_out_weights():
+        for step in range(nz):
+            take_weights(1, toward(step))
+
+    def mix_rows(xx, cc):
+        return pl.ds(pl.multiple_of((xx * CORES + cc) * count, count), count)
+
+    def emit(turn):
+        for piece in range(PIECES):
+            m.part[...] = dot_nn(m.mix[...], m.out_w[:, piece * slab : (piece + 1) * slab])
+            for slot, side in enumerate((nx, x)):
+                m.core_out[slot, turn, piece] = m.part[mix_rows(side, nc), :].astype(bf)
+                core_copy(slot, turn, piece).start()
+            for slot, side in enumerate((nx, x)):
+                m.keep[slot, turn, piece] = m.part[mix_rows(side, c), :]
+
+    def to_x(turn, carry):
+        for piece in range(PIECES):
+            core_copy(0, turn, piece).wait_recv()
+            total = m.keep[0, turn, piece] + m.core_in[0, turn, piece].astype(f32)
+            m.x_out[turn, piece] = total.astype(bf)
+            x_copy(turn, piece).start()
+        return carry
+
+    for step in range(PAIR, nz):
+        pass_weights(1, step)
 
     @pl.when(is_ret)
     def _():
@@ -952,7 +1062,8 @@
                 m.before[zz, yy] = running
                 running = running * jnp.exp(totals[zz * SIDES + yy]) + m.states[zz, yy].astype(f32)
 
-        def finish_run(zz, carry):
+        def finish_run(turn, carry):
+            zz = home(turn)
             rows = run_rows(zz)
             query = (m.queries[rows, 0:key_size].astype(f32) * m.fade_q[rows, :]).astype(bf)
             state = m.before[zz, y]
@@ -960,23 +1071,23 @@
             low = (state - high.astype(f32)).astype(bf)
             total = m.inner[rows, :] + (dot_nn(query, high) + dot_nn(query, low))
             total = total * lax.rsqrt(jnp.mean(total * total, axis=-1, keepdims=True) + epsilon)
-            total = total.astype(bf)
-            for xx in range(2):
-                store_mix(zz, xx, slice(0, V_DIM), total[xx * WINDOW : (xx + 1) * WINDOW])
+            m.mix[...] = total.astype(bf)
+            emit(turn)
             return carry
 
+        take_out_weights()
         lax.fori_loop(0, nz, finish_run, 0)
+        lax.fori_loop(0, nz, to_x, 0)
         for zz in range(nz):
             state_copy(zz).wait_send()
 
     @pl.when(is_att)
     def _():
-        halo_copy.wait_recv()
-        for zz in range(nz):
-            place(zz, 0, m.halo[jnp.maximum(zz - 1 + y, 0)])
         row = lax.broadcasted_iota(jnp.int32, (WINDOW, 2 * WINDOW), 0)
         column = lax.broadcasted_iota(jnp.int32, (WINDOW, 2 * WINDOW), 1)
         band = (column > row) & (column <= row + WINDOW)
+        m.bias[0] = jnp.where(band & (column >= WINDOW), 0.0, masked_out)
+        m.bias[1] = jnp.where(band, 0.0, masked_out)
         sink_row = m.aux[sp, parts : parts + 1, 0:LANES]
         sink_lane = lax.broadcasted_iota(jnp.int32, (1, LANES), 1)
         heads = V_DIM // HEAD_DIM
@@ -986,118 +1097,86 @@
             )
             for head in range(heads)
         ]
-
-        def attend_run(zz, carry):
+        halo_copy.wait_recv()
+        for zz in range(nz):
+            place(zz, 0, m.halo[jnp.maximum(zz - 1 + y, 0)])
+        take_out_weights()
+
+        def attend_run(turn, carry):
+            zz = home(turn)
             for xx in range(2):
-                first = (zz + y + xx) == 0
-                allowed = band & ((column >= WINDOW) | jnp.logical_not(first))
+                bias = m.bias[jnp.minimum(zz + y + xx, 1)]
                 where = pl.ds(xx * WINDOW, 2 * WINDOW)
                 rows = pl.ds(pl.multiple_of(zz * length + xx * WINDOW, WINDOW), WINDOW)
                 for pair in range(heads // 2):
                     lanes = slice(pair * LANES, (pair + 1) * LANES)
                     query = m.queries[rows, lanes]
-                    mixed = None
+                    terms, ends = [], []
                     for side in range(2):
                         sink = sinks[pair * 2 + side]
-                        scores = dot_nt(query, m.kv[side, zz, where, :]) * HEAD_DIM ** (-0.5)
-                        scores = jnp.where(allowed, scores, masked_out)
+                        scores = dot_nt(query, m.kv[side, zz, where, :]) + bias
                         highest = jnp.maximum(jnp.max(scores, axis=-1, keepdims=True), sink)
-                        lifted = jnp.exp(scores - highest)
-                        below = jnp.sum(lifted, axis=-1, keepdims=True) + jnp.exp(sink - highest)
-                        weights = (lifted / below).astype(bf)
-                        term = dot_nn(weights, m.kv[2 + side, zz, where, :])
-                        mixed = term if mixed is None else mixed + term
-                    store_mix(zz, xx, lanes, mixed.astype(bf))
+                        lifted = jnp.exp(scores - highest).astype(bf)
+                        ends.append(jnp.exp(sink - highest))
+                        terms.append(dot_nn(lifted, m.kv[2 + side, zz, where, :]))
+                    first = lane_kv < HEAD_DIM
+                    below = pltpu.roll(jnp.where(first, terms[1], terms[0]), HEAD_DIM, 1)
+                    below = below + jnp.where(first, ends[0], ends[1])
+                    mixed = jnp.where(first, terms[0], terms[1]) / below
+                    m.mix[xx * WINDOW : (xx + 1) * WINDOW, lanes] = mixed.astype(bf)
+            emit(turn)
+            to_x(turn, carry)
             return carry
 
         lax.fori_loop(0, nz, attend_run, 0)
         halo_copy.wait_send()
 
-    for step in range(nz):
-        take_weights(1, around(step))
-
-    def mix_rows(xx, cc):
-        return pl.ds(pl.multiple_of((xx * CORES + cc) * group, group), group)
-
-    def core_copy(slot, q):
-        return remote(
-            m.core_out.at[slot, q], m.core_in.at[slot, q], m.rc_s.at[slot, q], m.rc_r.at[slot, q],
-            device(z, y, x, nc),
-        )
-
-    def x_copy(q):
-        return remote(m.x_out.at[q], m.x_in.at[q], m.rx_s.at[q], m.rx_r.at[q], device(z, y, nx, c))
-
-    def home_rows(zz):
-        return pl.ds(pl.multiple_of(zz * count, count), count)
-
-    def z_copy(q, zz):
-        return remote(
-            m.z_out.at[q, home_rows(zz)], m.z_in.at[q, z], m.rz_s.at[q, zz], m.rz_r.at[q, z],
-            device(zz, y, x, c),
-        )
-
-    def z_arrival(q, zz):
-        return remote(
-            m.z_out.at[q, home_rows(zz)], m.z_in.at[q, zz], m.rz_s.at[q, zz], m.rz_r.at[q, zz],
-            device(zz, y, x, c),
-        )
-
-    def to_core(slot, xx):
-        def body(q, carry):
-            m.core_out[slot, q] = dot_nn(m.mix[mix_rows(xx, nc), :], m.out_w[q]).astype(bf)
-            core_copy(slot, q).start()
-            return carry
-
-        lax.fori_loop(0, n, body, 0)
-
-    to_core(0, nx)
-
-    def to_x(q, carry):
-        own = dot_nn(m.mix[mix_rows(nx, c), :], m.out_w[q])
-        core_copy(0, q).wait_recv()
-        m.x_out[q] = (own + m.core_in[0, q].astype(f32)).astype(bf)
-        x_copy(q).start()
-        return carry
-
-    lax.fori_loop(0, n, to_x, 0)
-    to_core(1, x)
-
-    def to_z(q, carry):
-        own = dot_nn(m.mix[mix_rows(x, c), :], m.out_w[q])
-        core_copy(1, q).wait_recv()
-        own = own + m.core_in[1, q].astype(f32)
-        x_copy(q).wait_recv()
-        own = own + m.x_in[q].astype(f32)
-        m.acc[q] = own
-        m.z_out[q] = own.astype(bf)
-        for step in range(1, nz):
-            z_copy(q, around(step)).start()
-        return carry
-
-    lax.fori_loop(0, n, to_z, 0)
-    for q in range(n):
-        total = m.acc[q, home_rows(z), :]
-        for step in range(1, nz):
-            z_arrival(q, around(step)).wait_recv()
-            total = total + m.z_in[q, around(step)].astype(f32)
-        out_ref[:, q * width : (q + 1) * width] = total.astype(bf)
+    outer = (z == 0) | (z == nz - 1)
+
+    def to_z(turn):
+        for piece in range(PIECES):
+            core_copy(1, turn, piece).wait_recv()
+            x_copy(turn, piece).wait_recv()
+            total = m.keep[1, turn, piece] + m.core_in[1, turn, piece].astype(f32)
+            total = total + m.x_in[turn, piece].astype(f32)
+            if turn < PAIR:
+
+                @pl.when(outer)
+                def _():
+                    m.z_out[turn, piece] = total.astype(bf)
+                    z_copy(turn, piece, mate, turn).start()
+
+                @pl.when(jnp.logical_not(outer))
+                def _():
+                    z_copy(turn, piece, mate, turn).wait_recv()
+                    merged = total + m.z_in[turn, piece].astype(f32)
+                    m.z_out[turn, piece] = merged.astype(bf)
+                    z_copy(turn, piece, home(turn), nz - 1).start()
+            elif turn < nz - 1:
+                m.z_out[turn, piece] = total.astype(bf)
+                z_copy(turn, piece, mate, turn).start()
+            else:
+                z_copy(nz - 2, piece, mate, nz - 2).wait_recv()
+                total = total + m.z_in[nz - 2, piece].astype(f32)
+                z_copy(0, piece, mate, nz - 1).wait_recv()
+                total = total + m.z_in[nz - 1, piece].astype(f32)
+                out_ref[:, piece * slab : (piece + 1) * slab] = total.astype(bf)
+
+    for turn in range(nz):
+        to_z(turn)
 
     for copy, condition in started:
         if condition is None:
             copy.wait_send()
         else:
             pl.when(condition)(copy.wait_send)
-
-    def drain(q, carry):
-        for slot in range(2):
-            core_copy(slot, q).wait_send()
-        x_copy(q).wait_send()
-        for step in range(1, nz):
-            z_copy(q, around(step)).wait_send()
-        return carry
-
-    lax.fori_loop(0, n, drain, 0)
+    for turn in range(nz):
+        for piece in range(PIECES):
+            for slot in range(2):
+                core_copy(slot, turn, piece).wait_send()
+            x_copy(turn, piece).wait_send()
+            if turn < nz - 1:
+                z_copy(turn, piece, mate, turn).wait_send()
 
 
 def layer(n, n_tp, tokens, norm_gain, aux, *weights):
@@ -1109,7 +1188,7 @@
     return pl.pallas_call(
         functools.partial(layer_kernel, n, n_tp, tuple(scratch)),
         out_shape=jax.ShapeDtypeStruct((count, n * width), jnp.bfloat16),
-        in_specs=[vmem] * (3 + len(weights)),
+        in_specs=[pl.BlockSpec(memory_space=pltpu.HBM)] * (3 + len(weights)),
         out_specs=vmem,
         scratch_shapes=list(scratch.values()),
         compiler_params=pltpu.CompilerParams(
@@ -1149,7 +1228,7 @@
         )
         return layer(
             n, n_tp, tokens, norm_gain, aux,
-            ret_query, ret_key, ret_value, att_query, att_key, att_value, ret_out, att_out,
+            ret_query, ret_key, ret_value, att_query, att_key.T, att_value.T, ret_out, att_out,
         )
     tok_float = tokens.astype(jnp.float32)
     normed = (

time: 117 us -> 99.8 us (0.85)
  Pallas kernels: 112 us -> 96.6 us
  local copies, waits for them, and re-layouts: 4.59 us -> 2.35 us
    pallas_call x1, Pallas kernels: 112 us -> 96.6 us  [layer(): pl.pallas_call(functools.partial(layer_kernel, n, n_tp, tuple(scratch)),...]
    unnamed x9 -> x5, local copies, waits for them, and re-layouts: 4.59 us -> 2.35 us
where the time goes in v2:
time: 99.8 us; the launch traced here: 99.6 us
  Pallas kernels  96.6 us (97%)
  local copies, waits for them, and re-layouts  2.35 us (2%)
    pallas_call x1, Pallas kernels, layer(): pl.pallas_call(functools.partial(layer_kernel, n, n_tp, tuple(scratch)),...  96.6 us
    unnamed x5, local copies, waits for them, and re-layouts  2.35 us

profile of v2, /device:TPU:0, one launch (start us, length us, event | category | flops | bytes accessed | tf_op | source)
XLA Modules:
  0.0 99.6 jit_solution(9915094286262328892)
XLA Ops:
  0.0 0.0 copy-start
  0.0 0.0 copy-start.1
  0.0 0.7 copy-done
  0.7 0.0 copy-done.1
  0.7 0.6 select_maximum_fusion.refs_2_
  1.3 96.6 %layer.1 = bf16[64,2048]{1,0:T(8,128)(2,1)} custom-call(bf16[64,2048]{1,0:T(8,128)(2,1)} %refs_0_.1, f32[1,2048]{1,0:T(1,128)} %bitcast.7, f32[8,256]{1,0:T(8,128)} %select_maximum_fusion.refs_2_, bf16[256,256]{1,0:T(8,128)(2,1)} %refs_3_.1, bf16[256,256]{1,0:T(8,128)(2,1)} %refs_4_.1, bf16[256,512]{1,0:T(8,128)(2,1)} %refs_5_.1, bf16[256,512]{1,0:T(8,128)(2,1)} %refs_6_.1, ...), custom_call_target="tpu_custom_call" | custom-call | flops 4294967296 | bytes 16777216 | tf_op jit(solution)/shard_map/layer/pallas_call | solution.py:1188
  97.9 1.7 %copy.14 = bf16[64,2048]{1,0:T(8,128)(2,1)} copy(bf16[64,2048]{1,0:T(8,128)(2,1)} %layer.1) | data formatting | bytes 524288
Async XLA Ops:
  0.0 0.7 copy-start
  0.0 0.7 copy-start.1

commit v3 on v2

--- a/solution.py
+++ b/solution.py
@@ -512,10 +512,22 @@
     )(*mixes, *weights)
 
 
+ORDER = (
+    "s0a", "S0a", "s1a", "T", "p0", "t1", "s2a", "a", "p1", "D", "P0", "t2", "x0", "f2a", "s3a", "c0",
+    "k0", "m00", "x1", "p2", "t3", "p3", "f3a", "S1a", "S2a", "S3a", "c1", "k1", "m01", "m10", "m11",
+    "x2", "x3", "u0", "v0", "c2", "m02", "m12", "c3", "m03", "m13", "P1", "u1", "k2", "m20", "m21",
+    "m22", "m23", "k3", "m30", "m31", "m32", "m33",
+)
+AFTER = (
+    "P2", "u2", "P3", "u3", "v1",
+)
 SIDES = 2
 CORES = 2
 PAIR = 2
-PIECES = 2
+SLICES = 4
+SHARES = 1
+OUT = SHARES
+SMALL = SHARES + 1
 
 
 def layer_fits(n, n_tp, shapes):
@@ -541,7 +553,7 @@
     nz = n // SIDES
     length = n_tp * count
     rows = nz * length
-    slab = n * width // PIECES
+    slab = SIDES * width
     att_width = V_DIM + 2 * HEAD_DIM
     ret_width = 2 * RETAIN_KEY_SIZE + V_DIM
     parts = nz // CORES
@@ -557,10 +569,13 @@
         out_w=pltpu.VMEM((V_DIM, n * width), bf),
         tokens=pltpu.VMEM((count, features), bf),
         gain=pltpu.VMEM((1, features), f32),
+        logs=pltpu.VMEM((parts, length), f32),
+        sinks=pltpu.VMEM((1, parts * V_DIM // HEAD_DIM), f32),
         aux_here=pltpu.VMEM((8, length), f32),
         kv_pack=pltpu.VMEM((2 * HEAD_DIM, depth), bf),
         bias=pltpu.VMEM((2, WINDOW, 2 * WINDOW), f32),
         aux=pltpu.VMEM((n, 8, length), f32),
+        total=pltpu.VMEM((rows, ret_width), f32),
         cosine=pltpu.VMEM((rows, RETAIN_KEY_SIZE), f32),
         sine=pltpu.VMEM((rows, RETAIN_KEY_SIZE), f32),
         fade_q=pltpu.VMEM((rows, RETAIN_KEY_SIZE), f32),
@@ -575,36 +590,41 @@
         kv=pltpu.VMEM((4, nz, length + WINDOW, 2 * HEAD_DIM), bf),
         rim=pltpu.VMEM((nz, WINDOW, 2 * HEAD_DIM), bf),
         halo=pltpu.VMEM((nz, WINDOW, 2 * HEAD_DIM), bf),
-        mix=pltpu.VMEM((length, V_DIM), bf),
-        part=pltpu.VMEM((length, slab), f32),
-        keep=pltpu.VMEM((2, nz, PIECES, count, slab), f32),
-        core_out=pltpu.VMEM((2, nz, PIECES, count, slab), bf),
-        core_in=pltpu.VMEM((2, nz, PIECES, count, slab), bf),
-        x_out=pltpu.VMEM((nz, PIECES, count, slab), bf),
-        x_in=pltpu.VMEM((nz, PIECES, count, slab), bf),
-        z_out=pltpu.VMEM((nz, PIECES, count, slab), bf),
-        z_in=pltpu.VMEM((nz, PIECES, count, slab), bf),
+        mix_far=pltpu.VMEM((nz, WINDOW, V_DIM), bf),
+        mix_near=pltpu.VMEM((nz, WINDOW, V_DIM), bf),
+        mix_in=pltpu.VMEM((nz, WINDOW, V_DIM), bf),
+        out_wx=pltpu.VMEM((V_DIM, n * width), bf),
+        part=pltpu.VMEM((WINDOW, slab), f32),
+        result=pltpu.VMEM((count, n * width), bf),
+        keep=pltpu.VMEM((nz, nz, count, slab), f32),
+        core_out=pltpu.VMEM((nz, nz, count, slab), bf),
+        core_in=pltpu.VMEM((nz, nz, count, slab), bf),
+        z_out=pltpu.VMEM((nz, nz, count, slab), bf),
+        z_in=pltpu.VMEM((nz, nz, count, slab), bf),
         tz_s=dma((2, nz)),
-        tz_r=dma((nz,)),
+        tz_r=dma((nz, SLICES)),
         tx_s=dma((nz,)),
-        tx_r=dma((nz,)),
+        tx_r=dma((nz, SLICES)),
         tc_s=dma((nz, 2)),
         tc_r=dma((nz, 2)),
-        w_s=dma((3, nz, CORES)),
-        w_r=dma((3, nz)),
-        f_s=dma((3, nz)),
-        f_r=dma((3, nz)),
+        w_s=dma((SHARES + 2, nz, CORES)),
+        w_r=dma((SHARES + 2, nz)),
+        f_s=dma((SHARES + 2, nz)),
+        f_r=dma((SHARES + 2, nz)),
         s_s=dma((nz,)),
         s_r=dma((nz,)),
         h_s=dma((1,)),
         h_r=dma((1,)),
-        rc_s=dma((2, nz, PIECES)),
-        rc_r=dma((2, nz, PIECES)),
-        rx_s=dma((nz, PIECES)),
-        rx_r=dma((nz, PIECES)),
-        rz_s=dma((nz, PIECES)),
-        rz_r=dma((nz, PIECES)),
-        load=dma((16,)),
+        ox_s=dma((1,)),
+        ox_r=dma((nz, SIDES)),
+        rc_s=dma((1,)),
+        rc_r=dma((nz, nz)),
+        rx_s=dma((1,)),
+        rx_r=dma((nz,)),
+        rz_s=dma((1,)),
+        rz_r=dma((nz, nz)),
+        load=dma((8,)),
+        store=dma((1,)),
     )
 
 
@@ -627,16 +647,16 @@
 
 
 def layer_kernel(n, n_tp, names, *refs):
-    (tokens_ref, gain_ref, aux_ref, rq_ref, rk_ref, rv_ref, aq_ref, ak_ref, av_ref, ro_ref, ao_ref) = refs[:11]
-    out_ref = refs[11]
-    m = Named(names, refs[12:])
+    (tokens_ref, gain_ref, logs_ref, sinks_ref, rq_ref, rk_ref, rv_ref, aq_ref, ak_ref, av_ref, ro_ref, ao_ref) = refs[:12]
+    out_ref = refs[12]
+    m = Named(names, refs[13:])
     nz = n // SIDES
     parts = nz // CORES
     count, features = tokens_ref.shape
     depth = rq_ref.shape[0]
     width = out_ref.shape[1] // n
     length = n_tp * count
-    slab = out_ref.shape[1] // PIECES
+    slab = SIDES * width
     key_size = RETAIN_KEY_SIZE
     bf, f32 = jnp.bfloat16, jnp.float32
 
@@ -686,22 +706,29 @@
         else:
             pl.when(condition)(copy.wait_recv)
 
-    moves = [(tokens_ref, m.tokens), (gain_ref, m.gain), (aux_ref, m.aux_here)]
-    moves += [(ak_ref, m.kv_pack.at[0:HEAD_DIM]), (av_ref, m.kv_pack.at[HEAD_DIM:])]
+    moves = [
+        (tokens_ref, m.tokens, 0),
+        (gain_ref, m.gain, 1),
+        (logs_ref, m.logs, 2),
+        (sinks_ref, m.sinks, 3),
+        (ak_ref, m.kv_pack.at[0:HEAD_DIM], 4),
+        (av_ref, m.kv_pack.at[HEAD_DIM:], 4),
+    ]
     for part in range(parts):
         wide = slice(part * V_DIM, (part + 1) * V_DIM)
         thin = slice(part * key_size, (part + 1) * key_size)
         moves += [
-            (rq_ref.at[:, thin], m.ret_pack.at[part, :, 0:key_size]),
-            (rk_ref.at[:, thin], m.ret_pack.at[part, :, key_size : 2 * key_size]),
-            (rv_ref.at[:, wide], m.ret_pack.at[part, :, 2 * key_size :]),
-            (aq_ref.at[:, wide], m.att_pack.at[part, :, 0:V_DIM]),
+            (rq_ref.at[:, thin], m.ret_pack.at[part, :, 0:key_size], 5),
+            (rk_ref.at[:, thin], m.ret_pack.at[part, :, key_size : 2 * key_size], 5),
+            (rv_ref.at[:, wide], m.ret_pack.at[part, :, 2 * key_size :], 5),
+            (aq_ref.at[:, wide], m.att_pack.at[part, :, 0:V_DIM], 6),
         ]
-    moves += [(ro_ref, m.out_pack.at[0]), (ao_ref, m.out_pack.at[1])]
-    loads = []
-    for index, (src, dst) in enumerate(moves):
-        loads.append(pltpu.make_async_copy(src, dst, m.load.at[index]))
-        loads[-1].start()
+    moves += [(ro_ref, m.out_pack.at[0], 7), (ao_ref, m.out_pack.at[1], 7)]
+    for src, dst, index in moves:
+        pltpu.make_async_copy(src, dst, m.load.at[index]).start()
+
+    def loaded(piece, index):
+        pltpu.make_async_copy(piece, piece, m.load.at[index]).wait()
 
     barrier = pltpu.get_barrier_semaphore()
     peers = [device(z, ny, x, c), device(z, y, nx, c), device(z, y, x, nc)]
@@ -714,59 +741,93 @@
     def token_rows(zz, xx, cc):
         return pl.ds(pl.multiple_of(zz * length + xx * (CORES * count) + cc * count, count), count)
 
-    loads[0].wait()
-    loads[1].wait()
+    loaded(m.tokens, 0)
+    loaded(m.gain, 1)
     tok_float = m.tokens[...].astype(f32)
     scale = lax.rsqrt(jnp.mean(tok_float * tok_float, axis=-1, keepdims=True) + epsilon)
     m.tok[token_rows(z, x, c), :] = (tok_float * scale * m.gain[...]).astype(bf)
-    for copy in loads[2:]:
-        copy.wait()
+    loaded(m.logs, 2)
+    loaded(m.sinks, 3)
+    loaded(m.kv_pack, 4)
+    loaded(m.ret_pack, 5)
+    loaded(m.att_pack.at[:, :, 0:V_DIM], 6)
+    loaded(m.out_pack, 7)
+    many = m.sinks.shape[1]
+    m.aux_here[...] = jnp.zeros_like(m.aux_here)
+    m.aux_here[0:parts, :] = m.logs[...]
+    m.aux_here[parts : parts + 1, 0:many] = m.sinks[...]
     pair = jnp.transpose(m.kv_pack[...].astype(f32)).astype(bf)
     for part in range(parts):
         m.att_pack[part, :, V_DIM:] = pair
     pl.semaphore_wait(barrier, len(peers))
 
-    def token_at(zz, xx, cc):
-        return m.tok.at[token_rows(zz, xx, cc)]
-
-    def token_z(origin, way):
-        piece = token_at(origin, x, c)
-        return remote(piece, piece, m.tz_s.at[way, origin], m.tz_r.at[origin], device(z + 1 - 2 * way, y, x, c))
-
-    def token_x(origin, side):
-        piece = token_at(origin, side, c)
-        return remote(piece, piece, m.tx_s.at[origin], m.tx_r.at[origin], device(z, y, nx, c))
-
-    def token_core(origin, side, core):
-        piece = token_at(origin, side, core)
+    def token_at(zz, xx, cc, cut):
+        if cut is None:
+            return m.tok.at[token_rows(zz, xx, cc)]
+        wide = features // SLICES
+        return m.tok.at[token_rows(zz, xx, cc), cut * wide : (cut + 1) * wide]
+
+    def token_z(origin, way, cut=None):
+        piece = token_at(origin, x, c, cut)
+        return remote(
+            piece,
+            piece,
+            m.tz_s.at[way, origin],
+            m.tz_r.at[origin, 0 if cut is None else cut],
+            device(z + 1 - 2 * way, y, x, c),
+        )
+
+    def token_x(origin, side, cut=None):
+        piece = token_at(origin, side, c, cut)
+        return remote(
+            piece, piece, m.tx_s.at[origin], m.tx_r.at[origin, 0 if cut is None else cut], device(z, y, nx, c)
+        )
+
+    def token_core(origin, side, core, cut=None):
+        piece = token_at(origin, side, core, cut)
         return remote(piece, piece, m.tc_s.at[origin, side], m.tc_r.at[origin, side], device(z, y, x, nc))
 
+    def send_rows(maker, cut, condition, *place):
+        copy = maker(*place, cut)
+        if condition is None:
+            copy.start()
+        else:
+            pl.when(condition)(copy.start)
+        if cut == 0:
+            started.append((maker(*place), condition))
+
     can_go = (z < nz - 1, z > 0)
 
-    def spread(origin, way, condition):
-        go(token_z(origin, way), both(condition, can_go[way]))
-
-    def weight_rows(zz, yy):
-        return pl.ds(pl.multiple_of((zz * SIDES + yy) * depth, depth), depth)
+    def spread(origin, cut, condition, ways):
+        for way in ways:
+            send_rows(token_z, cut, both(condition, can_go[way]), origin, way)
+        send_rows(token_x, cut, condition, origin, x)
+        send_rows(token_core, cut, condition, origin, x, c)
+
+    def weight_rows(zz, yy, share):
+        start = (zz * SIDES + yy) * depth + share * (depth // SHARES)
+        return pl.ds(pl.multiple_of(start, depth // SHARES), depth // SHARES)
 
     near, distant = c == z // parts, c != z // parts
+    outer = (z == 0) | (z == nz - 1)
+    inside = jnp.logical_not(outer)
 
     def toward(step):
         return (z, mate, lax.rem(z + PAIR, nz), nz - 1 - z)[step]
 
-    def send_weights(step, kind):
+    def send_weights(step, kind, where=None):
         target_z = toward(step)
         part = lax.rem(target_z, parts)
-        valid = near if step < PAIR else distant
+        valid = both(near if step < PAIR else distant, where)
         first = len(started)
         for core in range(CORES):
             target = device(target_z, y, x, core)
-            pack, dest = (m.ret_pack, m.ret_w) if core == 0 else (m.att_pack, m.att_w)
-            rows = pl.ds(pl.multiple_of(part * V_DIM, V_DIM), V_DIM)
-            if kind == 0:
-                src = pack.at[part]
-            elif kind == 1:
-                src = m.out_pack.at[core, rows]
+            pack = m.ret_pack if core == 0 else m.att_pack
+            if kind < SHARES:
+                high = depth // SHARES
+                src = pack.at[part, kind * high : (kind + 1) * high]
+            elif kind == OUT:
+                src = m.out_pack.at[core, pl.ds(pl.multiple_of(part * V_DIM, V_DIM), V_DIM)]
             else:
                 src = m.aux_here
             dst = weight_piece(kind, z, y, core)
@@ -776,12 +837,7 @@
 
                 @pl.when(valid & (c == core))
                 def _():
-                    if kind == 0:
-                        dest[weight_rows(z, y), :] = pack[part]
-                    elif kind == 1:
-                        m.out_w[:, out_columns(z, y)] = m.out_pack[core, rows, :]
-                    else:
-                        m.aux[sp] = m.aux_here[...]
+                    dst[...] = src[...]
 
         return started[first:]
 
@@ -794,14 +850,14 @@
         return pl.ds(pl.multiple_of((zz * SIDES + yy) * width, width), width)
 
     def weight_piece(kind, zz, yy, core):
-        if kind == 0:
-            return (m.ret_w if core == 0 else m.att_w).at[weight_rows(zz, yy)]
-        if kind == 1:
+        if kind < SHARES:
+            return (m.ret_w if core == 0 else m.att_w).at[weight_rows(zz, yy, kind)]
+        if kind == OUT:
             return m.out_w.at[:, out_columns(zz, yy)]
         return m.aux.at[zz * SIDES + yy]
 
     def per_core(kind):
-        return ((0, is_ret), (1, is_att)) if kind == 0 else ((0, None),)
+        return ((0, is_ret), (1, is_att)) if kind < SHARES else ((0, None),)
 
     def pass_weights(kind, step):
         zz = toward(step)
@@ -825,101 +881,145 @@
             )
 
     for step in range(nz):
-        send_weights(step, 2)
-    for way in range(2):
-        spread(z, way, None)
-    go(token_x(z, x))
-    go(token_core(z, x, c))
-    for kind in range(2):
-        for step in range(PAIR):
-            send_weights(step, kind)
+        send_weights(step, SMALL)
+    for cut in range(SLICES):
+        spread(z, cut, None, (0, 1))
 
     def pass_tokens(step):
-        for way in range(2):
-            origin = z - step if way == 0 else z + step
-            valid = origin >= 0 if way == 0 else origin < nz
-            await_recv(token_z(origin, way), valid)
-            spread(origin, way, valid)
-            go(token_x(origin, x), valid)
-            go(token_core(origin, x, c), valid)
+        for cut in range(SLICES):
+            for way in range(2):
+                origin = z - step if way == 0 else z + step
+                valid = origin >= 0 if way == 0 else origin < nz
+                await_recv(token_z(origin, way, cut), valid)
+                spread(origin, cut, valid, (way,))
 
     def across_tokens(step):
         origin = toward(step)
-        await_recv(token_x(origin, nx))
-        go(token_core(origin, nx, c))
-
-    @pl.when(is_ret)
-    def _():
-        lane = lax.broadcasted_iota(jnp.int32, (length, key_size), 1)
-        row = lax.broadcasted_iota(jnp.int32, (length, key_size), 0)
-        half = key_size // 2
-        inverse = jnp.exp(
-            lax.rem(lane, half).astype(f32) * (-math.log(rope_base) / half)
-        )
-        sign = jnp.where(lane < half, -1.0, 1.0)
-
-        def table(zz, carry):
-            where = pl.ds(pl.multiple_of(zz * length, length), length)
-            angles = (row + (zz * SIDES + y) * length).astype(f32) * inverse
-            m.cosine[where, :] = jnp.cos(angles)
-            m.sine[where, :] = jnp.sin(angles) * sign
-            return carry
-
-        lax.fori_loop(0, nz, table, 0)
-
-    pass_weights(0, 0)
-    pass_tokens(1)
-    second = send_weights(2, 0)
-    for step in range(nz):
-        pass_weights(2, step)
-    pass_weights(0, 1)
-    pass_weights(1, 0)
-    pass_tokens(2)
-    across_tokens(0)
-    pass_weights(1, 1)
-    finish(second)
-    third = send_weights(3, 0)
-    pass_tokens(3)
-    pass_weights(0, 2)
-    across_tokens(1)
-    finish(third)
-    send_weights(2, 1)
-    send_weights(3, 1)
-    pass_weights(0, 3)
-    across_tokens(3)
-    across_tokens(2)
-    for zz in range(nz):
-        take_weights(2, zz)
-
-    @pl.when(is_ret)
-    def _():
-        lower = (
-            lax.broadcasted_iota(jnp.int32, (length, length), 0)
-            >= lax.broadcasted_iota(jnp.int32, (length, length), 1)
-        )
-        lower_float = lower.astype(f32)
-        mine = [m.aux[zz * SIDES + y, pl.ds(part_here, 1), :] for zz in range(nz)]
-        logs = jnp.concatenate(mine * (8 // nz), axis=0)
-        by_row = dot_nt(logs, lower_float, precision=lax.Precision.HIGHEST)
-        by_column = dot_nt(lower_float, logs, precision=lax.Precision.HIGHEST)
+        for cut in range(SLICES):
+            await_recv(token_x(origin, nx, cut))
+            send_rows(token_core, cut, None, origin, nx, c)
+
+    def tables():
+        @pl.when(is_ret)
+        def make_tables():
+            lane = lax.broadcasted_iota(jnp.int32, (length, key_size), 1)
+            row = lax.broadcasted_iota(jnp.int32, (length, key_size), 0)
+            half = key_size // 2
+            inverse = jnp.exp(
+                lax.rem(lane, half).astype(f32) * (-math.log(rope_base) / half)
+            )
+            sign = jnp.where(lane < half, -1.0, 1.0)
+
+            def table(zz, carry):
+                where = pl.ds(pl.multiple_of(zz * length, length), length)
+                angles = (row + (zz * SIDES + y) * length).astype(f32) * inverse
+                m.cosine[where, :] = jnp.cos(angles)
+                m.sine[where, :] = jnp.sin(angles) * sign
+                return carry
+
+            lax.fori_loop(0, nz, table, 0)
+
+    def decays():
         for zz in range(nz):
-            rows = slice(zz * length, (zz + 1) * length)
-            column = by_column[:, zz : zz + 1]
-            closing = by_column[length - 1 : length, zz : zz + 1]
-            within = jnp.minimum(column - by_row[zz : zz + 1, :], 0.0)
-            m.decay[rows, :] = jnp.where(lower, jnp.exp(within), 0.0)
-            m.fade_q[rows, :] = jnp.broadcast_to(jnp.exp(column), (length, key_size))
-            m.fade_k[rows, :] = jnp.broadcast_to(jnp.exp(closing - column), (length, key_size))
-
-    for step in range(nz):
-        take_weights(0, toward(step))
-    for step in range(nz):
+            take_weights(SMALL, zz)
+
+        @pl.when(is_ret)
+        def _():
+            lower = (
+                lax.broadcasted_iota(jnp.int32, (length, length), 0)
+                >= lax.broadcasted_iota(jnp.int32, (length, length), 1)
+            )
+            lower_float = lower.astype(f32)
+            mine = [m.aux[zz * SIDES + y, pl.ds(part_here, 1), :] for zz in range(nz)]
+            logs = jnp.concatenate(mine * (8 // nz), axis=0)
+            by_row = dot_nt(logs, lower_float, precision=lax.Precision.HIGHEST)
+            by_column = dot_nt(lower_float, logs, precision=lax.Precision.HIGHEST)
+            for zz in range(nz):
+                rows = slice(zz * length, (zz + 1) * length)
+                column = by_column[:, zz : zz + 1]
+                closing = by_column[length - 1 : length, zz : zz + 1]
+                within = jnp.minimum(column - by_row[zz : zz + 1, :], 0.0)
+                m.decay[rows, :] = jnp.where(lower, jnp.exp(within), 0.0)
+                m.fade_q[rows, :] = jnp.broadcast_to(jnp.exp(column), (length, key_size))
+                m.fade_k[rows, :] = jnp.broadcast_to(jnp.exp(closing - column), (length, key_size))
+
+    def run_rows(zz):
+        return pl.ds(pl.multiple_of(zz * length, length), length)
+
+    def take_tokens(step):
         origin = toward(step)
         for side in (x, nx):
             await_recv(token_core(origin, side, nc))
 
-    def run_rows(zz):
-        return pl.ds(pl.multiple_of(zz * length, length), length)
+    def out_x(step, side):
+        columns = out_columns(toward(step), side)
+        return remote(
+            m.out_w.at[:, columns],
+            m.out_wx.at[:, columns],
+            m.ox_s.at[0],
+            m.ox_r.at[step, side],
+            device(z, y, nx, c),
+        )
+
+    fresh = set()
+
+    def project(step, run):
+        columns = pl.ds(pl.multiple_of(toward(step) * SIDES * depth, SIDES * depth), SIDES * depth)
+        rows = run_rows(toward(run))
+        first = run not in fresh
+        fresh.add(run)
+
+        def accumulate(held):
+            lanes = slice(0, held.shape[1])
+            product = dot_nn(m.tok[rows, columns], held[columns, :])
+            m.total[rows, lanes] = product if first else m.total[rows, lanes] + product
+
+        pl.when(is_ret)(lambda: accumulate(m.ret_w))
+        pl.when(is_att)(lambda: accumulate(m.att_w))
+
+    everyone = dict(a=None, o=outer, i=inside)
+    sent = {}
+    def perform(word):
+        step = int(word[1]) if len(word) > 1 else 0
+        if word[0] == "s":
+            for kind in range(SHARES):
+                sent[word, kind] = send_weights(step, kind, everyone[word[2]])
+        elif word[0] == "f":
+            for kind in range(SHARES):
+                finish(sent["s" + word[1:], kind])
+        elif word[0] == "p":
+            for kind in range(SHARES):
+                pass_weights(kind, step)
+        elif word[0] == "S":
+            sent[word] = send_weights(step, OUT, everyone[word[2]])
+        elif word[0] == "P":
+            pass_weights(OUT, step)
+        elif word[0] == "t":
+            pass_tokens(step)
+        elif word[0] == "x":
+            across_tokens(step)
+        elif word[0] == "u":
+            out_x(step, y).start()
+        elif word[0] == "v":
+            take_weights(OUT, toward(step))
+            out_x(step, ny).start()
+        elif word[0] == "c":
+            take_tokens(step)
+        elif word[0] == "k":
+            for kind in range(SHARES):
+                take_weights(kind, toward(step))
+        elif word[0] == "m":
+            project(step, int(word[2]))
+        elif word[0] == "T":
+            tables()
+        elif word[0] == "D":
+            decays()
+        elif word[0] == "a":
+            for aux_step in range(nz):
+                pass_weights(SMALL, aux_step)
+
+    for word in ORDER:
+        perform(word)
 
     def state_copy(zz):
         piece = m.states.at[zz, y]
@@ -935,7 +1035,7 @@
     def _():
         def project_run(zz, carry):
             rows = run_rows(zz)
-            product = dot_nn(m.tok[rows, :], m.ret_w[...]).astype(bf)
+            product = m.total[rows, :].astype(bf)
             cosine, sine = m.cosine[rows, :], m.sine[rows, :]
 
             def turn(values):
@@ -970,7 +1070,7 @@
     def _():
         def project_run(zz, carry):
             rows = run_rows(zz)
-            product = dot_nn(m.tok[rows, :], m.att_w[...]).astype(bf)
+            product = m.total[rows, 0 : m.att_w.shape[1]].astype(bf)
             m.queries[rows, :] = (product[:, 0:V_DIM].astype(f32) * HEAD_DIM ** (-0.5)).astype(bf)
             for spot in range(2):
                 place(zz, spot + 1, product[spot * WINDOW : (spot + 1) * WINDOW, V_DIM:])
@@ -988,59 +1088,93 @@
             return (far, near, mate, z)[turn]
         return jnp.where(turn == 0, far, jnp.where(turn == 1, near, jnp.where(turn == 2, mate, z)))
 
-    def core_copy(slot, turn, piece):
+    def core_copy(turn, piece):
         return remote(
-            m.core_out.at[slot, turn, piece],
-            m.core_in.at[slot, turn, piece],
-            m.rc_s.at[slot, turn, piece],
-            m.rc_r.at[slot, turn, piece],
+            m.core_out.at[turn, piece],
+            m.core_in.at[turn, piece],
+            m.rc_s.at[0],
+            m.rc_r.at[turn, piece],
             device(z, y, x, nc),
         )
 
-    def x_copy(turn, piece):
+    def mix_copy(turn):
         return remote(
-            m.x_out.at[turn, piece],
-            m.x_in.at[turn, piece],
-            m.rx_s.at[turn, piece],
-            m.rx_r.at[turn, piece],
-            device(z, y, nx, c),
+            m.mix_far.at[turn], m.mix_in.at[turn], m.rx_s.at[0], m.rx_r.at[turn], device(z, y, nx, c)
         )
 
     def z_copy(turn, piece, target_z, slot):
+        spot = toward(piece)
         return remote(
-            m.z_out.at[turn, piece],
-            m.z_in.at[slot, piece],
-            m.rz_s.at[turn, piece],
-            m.rz_r.at[slot, piece],
+            m.z_out.at[turn, spot],
+            m.z_in.at[slot, spot],
+            m.rz_s.at[0],
+            m.rz_r.at[slot, spot],
             device(target_z, y, x, c),
         )
 
-    def take_out_weights():
-        for step in range(nz):
-            take_weights(1, toward(step))
-
-    def mix_rows(xx, cc):
-        return pl.ds(pl.multiple_of((xx * CORES + cc) * count, count), count)
-
-    def emit(turn):
-        for piece in range(PIECES):
-            m.part[...] = dot_nn(m.mix[...], m.out_w[:, piece * slab : (piece + 1) * slab])
-            for slot, side in enumerate((nx, x)):
-                m.core_out[slot, turn, piece] = m.part[mix_rows(side, nc), :].astype(bf)
-                core_copy(slot, turn, piece).start()
-            for slot, side in enumerate((nx, x)):
-                m.keep[slot, turn, piece] = m.part[mix_rows(side, c), :]
-
-    def to_x(turn, carry):
-        for piece in range(PIECES):
-            core_copy(0, turn, piece).wait_recv()
-            total = m.keep[0, turn, piece] + m.core_in[0, turn, piece].astype(f32)
-            m.x_out[turn, piece] = total.astype(bf)
-            x_copy(turn, piece).start()
-        return carry
-
-    for step in range(PAIR, nz):
-        pass_weights(1, step)
+    def half_rows(cc):
+        return pl.ds(pl.multiple_of(cc * count, count), count)
+
+    def slab_columns(piece):
+        return pl.ds(pl.multiple_of(toward(piece) * slab, slab), slab)
+
+    def block_rows(zz, xx):
+        return pl.ds(pl.multiple_of(zz * length + xx * WINDOW, WINDOW), WINDOW)
+
+    def take_out(piece):
+        for side in (y, ny):
+            out_x(piece, side).wait_recv()
+
+    def emit(turn, piece):
+        columns = slab_columns(piece)
+        m.part[...] = dot_nn(m.mix_near[turn], m.out_w[:, columns]) + dot_nn(
+            m.mix_in[turn], m.out_wx[:, columns]
+        )
+        m.core_out[turn, piece] = m.part[half_rows(nc), :].astype(bf)
+        core_copy(turn, piece).start()
+        m.keep[turn, piece] = m.part[half_rows(c), :]
+
+    def joined(turn, piece):
+        core_copy(turn, piece).wait_recv()
+        return m.keep[turn, piece] + m.core_in[turn, piece].astype(f32)
+
+    def pass_sum(turn, piece):
+        m.z_out[turn, toward(piece)] = joined(turn, piece).astype(bf)
+        z_copy(turn, piece, mate, turn).start()
+
+    def merge_sum(turn, piece):
+        z_copy(turn, piece, mate, turn).wait_recv()
+        merged = joined(turn, piece) + m.z_in[turn, toward(piece)].astype(f32)
+        m.z_out[turn, toward(piece)] = merged.astype(bf)
+        z_copy(turn, piece, home(turn), nz - 1).start()
+
+    def first_sums(turn, piece):
+        if turn < PAIR:
+            pl.when(outer)(lambda: pass_sum(turn, piece))
+        elif turn < nz - 1:
+            pass_sum(turn, piece)
+
+    early, late = (0, 1), (2, 3)
+
+    def rounds(block):
+        for turn in range(nz + 1):
+            if turn < nz:
+                block(turn)
+            if turn == 0:
+                perform("v2")
+            if turn == 1:
+                perform("v3")
+                for piece in early:
+                    take_out(piece)
+            if turn > 0:
+                mix_copy(turn - 1).wait_recv()
+                for piece in early:
+                    emit(turn - 1, piece)
+                for piece in early:
+                    first_sums(turn - 1, piece)
+
+    for word in AFTER:
+        perform(word)
 
     @pl.when(is_ret)
     def _():
@@ -1062,22 +1196,22 @@
                 m.before[zz, yy] = running
                 running = running * jnp.exp(totals[zz * SIDES + yy]) + m.states[zz, yy].astype(f32)
 
-        def finish_run(turn, carry):
-            zz = home(turn)
-            rows = run_rows(zz)
+        def finish_block(zz, xx):
+            rows = block_rows(zz, xx)
             query = (m.queries[rows, 0:key_size].astype(f32) * m.fade_q[rows, :]).astype(bf)
             state = m.before[zz, y]
             high = state.astype(bf)
             low = (state - high.astype(f32)).astype(bf)
             total = m.inner[rows, :] + (dot_nn(query, high) + dot_nn(query, low))
             total = total * lax.rsqrt(jnp.mean(total * total, axis=-1, keepdims=True) + epsilon)
-            m.mix[...] = total.astype(bf)
-            emit(turn)
-            return carry
-
-        take_out_weights()
-        lax.fori_loop(0, nz, finish_run, 0)
-        lax.fori_loop(0, nz, to_x, 0)
+            return total.astype(bf)
+
+        def both_blocks(turn):
+            m.mix_far[turn] = finish_block(home(turn), nx)
+            mix_copy(turn).start()
+            m.mix_near[turn] = finish_block(home(turn), x)
+
+        rounds(both_blocks)
         for zz in range(nz):
             state_copy(zz).wait_send()
 
@@ -1097,106 +1231,97 @@
             )
             for head in range(heads)
         ]
-        halo_copy.wait_recv()
-        for zz in range(nz):
-            place(zz, 0, m.halo[jnp.maximum(zz - 1 + y, 0)])
-        take_out_weights()
-
-        def attend_run(turn, carry):
-            zz = home(turn)
-            for xx in range(2):
-                bias = m.bias[jnp.minimum(zz + y + xx, 1)]
-                where = pl.ds(xx * WINDOW, 2 * WINDOW)
-                rows = pl.ds(pl.multiple_of(zz * length + xx * WINDOW, WINDOW), WINDOW)
-                for pair in range(heads // 2):
-                    lanes = slice(pair * LANES, (pair + 1) * LANES)
-                    query = m.queries[rows, lanes]
-                    terms, ends = [], []
-                    for side in range(2):
-                        sink = sinks[pair * 2 + side]
-                        scores = dot_nt(query, m.kv[side, zz, where, :]) + bias
-                        highest = jnp.maximum(jnp.max(scores, axis=-1, keepdims=True), sink)
-                        lifted = jnp.exp(scores - highest).astype(bf)
-                        ends.append(jnp.exp(sink - highest))
-                        terms.append(dot_nn(lifted, m.kv[2 + side, zz, where, :]))
-                    first = lane_kv < HEAD_DIM
-                    below = pltpu.roll(jnp.where(first, terms[1], terms[0]), HEAD_DIM, 1)
-                    below = below + jnp.where(first, ends[0], ends[1])
-                    mixed = jnp.where(first, terms[0], terms[1]) / below
-                    m.mix[xx * WINDOW : (xx + 1) * WINDOW, lanes] = mixed.astype(bf)
-            emit(turn)
-            to_x(turn, carry)
-            return carry
-
-        lax.fori_loop(0, nz, attend_run, 0)
+        def take_halo():
+            halo_copy.wait_recv()
+            for zz in range(nz):
+                place(zz, 0, m.halo[jnp.maximum(zz - 1 + y, 0)])
+
+        pl.when(x == 1)(take_halo)
+        def attend_block(zz, xx, target):
+            bias = m.bias[jnp.minimum(zz + y + xx, 1)]
+            where = pl.ds(pl.multiple_of(xx * WINDOW, WINDOW), 2 * WINDOW)
+            rows = block_rows(zz, xx)
+            first = lane_kv < HEAD_DIM
+            for pair in range(heads // 2):
+                lanes = slice(pair * LANES, (pair + 1) * LANES)
+                query = m.queries[rows, lanes]
+                terms, ends = [], []
+                for side in range(2):
+                    sink = sinks[pair * 2 + side]
+                    scores = dot_nt(query, m.kv[side, zz, where, :]) + bias
+                    highest = jnp.maximum(jnp.max(scores, axis=-1, keepdims=True), sink)
+                    lifted = jnp.exp(scores - highest).astype(bf)
+                    ends.append(jnp.exp(sink - highest))
+                    terms.append(dot_nn(lifted, m.kv[2 + side, zz, where, :]))
+                below = pltpu.roll(jnp.where(first, terms[1], terms[0]), HEAD_DIM, 1)
+                below = below + jnp.where(first, ends[0], ends[1])
+                mixed = jnp.where(first, terms[0], terms[1]) / below
+                target[:, lanes] = mixed.astype(bf)
+
+        def both_blocks(turn):
+            attend_block(home(turn), nx, m.mix_far.at[turn])
+            mix_copy(turn).start()
+            if turn == 0:
+                pl.when(x == 0)(take_halo)
+            attend_block(home(turn), x, m.mix_near.at[turn])
+
+        rounds(both_blocks)
         halo_copy.wait_send()
 
-    outer = (z == 0) | (z == nz - 1)
-
-    def to_z(turn):
-        for piece in range(PIECES):
-            core_copy(1, turn, piece).wait_recv()
-            x_copy(turn, piece).wait_recv()
-            total = m.keep[1, turn, piece] + m.core_in[1, turn, piece].astype(f32)
-            total = total + m.x_in[turn, piece].astype(f32)
-            if turn < PAIR:
-
-                @pl.when(outer)
-                def _():
-                    m.z_out[turn, piece] = total.astype(bf)
-                    z_copy(turn, piece, mate, turn).start()
-
-                @pl.when(jnp.logical_not(outer))
-                def _():
-                    z_copy(turn, piece, mate, turn).wait_recv()
-                    merged = total + m.z_in[turn, piece].astype(f32)
-                    m.z_out[turn, piece] = merged.astype(bf)
-                    z_copy(turn, piece, home(turn), nz - 1).start()
-            elif turn < nz - 1:
-                m.z_out[turn, piece] = total.astype(bf)
-                z_copy(turn, piece, mate, turn).start()
-            else:
-                z_copy(nz - 2, piece, mate, nz - 2).wait_recv()
-                total = total + m.z_in[nz - 2, piece].astype(f32)
-                z_copy(0, piece, mate, nz - 1).wait_recv()
-                total = total + m.z_in[nz - 1, piece].astype(f32)
-                out_ref[:, piece * slab : (piece + 1) * slab] = total.astype(bf)
-
-    for turn in range(nz):
-        to_z(turn)
+    def merge_sums(piece):
+        for turn in range(PAIR):
+            merge_sum(turn, piece)
+
+    for piece in early:
+        pl.when(inside)(functools.partial(merge_sums, piece))
+    for piece in late:
+        take_out(piece)
+        for turn in range(nz):
+            emit(turn, piece)
+        for turn in range(nz):
+            first_sums(turn, piece)
+    for piece in late:
+        pl.when(inside)(functools.partial(merge_sums, piece))
+    for piece in range(nz):
+        total = joined(nz - 1, piece)
+        for slot in (nz - 2, nz - 1):
+            z_copy(0, piece, mate, slot).wait_recv()
+            total = total + m.z_in[slot, toward(piece)].astype(f32)
+        columns = slab_columns(piece)
+        m.result[:, columns] = total.astype(bf)
+        pltpu.make_async_copy(m.result.at[:, columns], out_ref.at[:, columns], m.store.at[0]).start()
 
     for copy, condition in started:
         if condition is None:
             copy.wait_send()
         else:
             pl.when(condition)(copy.wait_send)
-    for turn in range(nz):
-        for piece in range(PIECES):
-            for slot in range(2):
-                core_copy(slot, turn, piece).wait_send()
-            x_copy(turn, piece).wait_send()
-            if turn < nz - 1:
-                z_copy(turn, piece, mate, turn).wait_send()
-
-
-def layer(n, n_tp, tokens, norm_gain, aux, *weights):
+    everything = device(z, y, x, nc)
+    remote(m.core_out, m.core_in, m.rc_s.at[0], m.rc_r.at[0, 0], everything).wait_send()
+    remote(m.mix_far, m.mix_in, m.rx_s.at[0], m.rx_r.at[0], everything).wait_send()
+    remote(m.out_w, m.out_wx, m.ox_s.at[0], m.ox_r.at[0, 0], everything).wait_send()
+    sums = m.z_out.at[0 : nz - 1]
+    remote(sums, sums, m.rz_s.at[0], m.rz_r.at[0, 0], everything).wait_send()
+    pltpu.make_async_copy(m.result, out_ref, m.store.at[0]).wait()
+
+
+def layer(n, n_tp, tokens, norm_gain, logs, sinks, *weights):
     count, features = tokens.shape
     depth = weights[0].shape[0]
     width = weights[-1].shape[1]
     scratch = layer_scratch(n, n_tp, count, features, depth, width)
-    vmem = pl.BlockSpec(memory_space=pltpu.VMEM)
     return pl.pallas_call(
         functools.partial(layer_kernel, n, n_tp, tuple(scratch)),
         out_shape=jax.ShapeDtypeStruct((count, n * width), jnp.bfloat16),
-        in_specs=[pl.BlockSpec(memory_space=pltpu.HBM)] * (3 + len(weights)),
-        out_specs=vmem,
+        in_specs=[pl.BlockSpec(memory_space=pltpu.HBM)] * (4 + len(weights)),
+        out_specs=pl.BlockSpec(memory_space=pltpu.HBM),
         scratch_shapes=list(scratch.values()),
         compiler_params=pltpu.CompilerParams(
             collective_id=3, has_side_effects=True, vmem_limit_bytes=60 * 2**20
         ),
         cost_estimate=pl.CostEstimate(flops=4 * 2**30, bytes_accessed=16 * 2**20, transcendentals=0),
         name="layer",
-    )(tokens, norm_gain.reshape(1, -1), aux, *weights)
+    )(tokens, norm_gain.reshape(1, -1), logs, sinks.reshape(1, -1), *weights)
 
 
 def on_device(
@@ -1223,11 +1348,8 @@
         length,
     )
     if layer_fits(n, n_tp, shapes):
-        aux = jnp.concatenate(
-            [log_decay, jnp.pad(sink_logits[None], ((0, 7 - log_decay.shape[0]), (0, length - sink_logits.shape[0])))], axis=0
-        )
         return layer(
-            n, n_tp, tokens, norm_gain, aux,
+            n, n_tp, tokens, norm_gain, log_decay, sink_logits,
             ret_query, ret_key, ret_value, att_query, att_key.T, att_value.T, ret_out, att_out,
         )
     tok_float = tokens.astype(jnp.float32)

time: 99.8 us -> 95.2 us (0.954)
  Pallas kernels: 96.6 us -> 93.3 us
    pallas_call x1, Pallas kernels: 96.6 us -> 93.3 us  [layer(): pl.pallas_call(functools.partial(layer_kernel, n, n_tp, tuple(scratch)),...]
    unnamed x5 -> x1, local copies, waits for them, and re-layouts: 2.35 us -> 1.67 us
where the time goes in v3:
time: 95.2 us; the launch traced here: 95 us
  Pallas kernels  93.3 us (98%)
  local copies, waits for them, and re-layouts  1.67 us (2%)
    pallas_call x1, Pallas kernels, layer(): pl.pallas_call(functools.partial(layer_kernel, n, n_tp, tuple(scratch)),...  93.3 us

profile of v3, /device:TPU:0, one launch (start us, length us, event | category | flops | bytes accessed | tf_op | source)
XLA Modules:
  0.0 95.0 jit_solution(3563616012030243851)
XLA Ops:
  0.0 93.3 %layer.1 = bf16[64,2048]{1,0:T(8,128)(2,1)} custom-call(bf16[64,2048]{1,0:T(8,128)(2,1)} %refs_0_.1, f32[1,2048]{1,0:T(1,128)} %bitcast.6, f32[2,256]{1,0:T(2,128)} %refs_2_.1, f32[1,8]{1,0:T(1,128)} %bitcast.7, bf16[256,256]{1,0:T(8,128)(2,1)} %refs_4_.1, bf16[256,256]{1,0:T(8,128)(2,1)} %refs_5_.1, bf16[256,512]{1,0:T(8,128)(2,1)} %refs_6_.1, ...), custom_call_target="tpu_custom_call" | custom-call | flops 4294967296 | bytes 16777216 | tf_op jit(solution)/shard_map/layer/pallas_call | solution.py:1313
  93.3 1.7 %copy.14 = bf16[64,2048]{1,0:T(8,128)(2,1)} copy(bf16[64,2048]{1,0:T(8,128)(2,1)} %layer.1) | data formatting | bytes 524288

commit v4 on v3

--- a/solution.py
+++ b/solution.py
@@ -513,14 +513,14 @@
 
 
 ORDER = (
-    "s0a", "S0a", "s1a", "T", "p0", "t1", "s2a", "a", "p1", "D", "P0", "t2", "x0", "f2a", "s3a", "c0",
-    "k0", "m00", "x1", "p2", "t3", "p3", "f3a", "S1a", "S2a", "S3a", "c1", "k1", "m01", "m10", "m11",
-    "x2", "x3", "u0", "v0", "c2", "m02", "m12", "c3", "m03", "m13", "P1", "u1", "k2", "m20", "m21",
+    "s0a", "S0a", "s1a", "T", "p0", "t1", "s2a", "a", "p1", "D", "P0", "t2", "x0", "f2a",
+    "s3a", "x1", "p2", "t3", "p3", "u0", "v0", "f3a", "S1a", "S2a", "S3a", "c0", "k0", "m00", "c1", "k1", "m01",
+    "m10", "m11", "x2", "x3", "c2", "m02", "m12", "c3", "m03", "m13", "P1", "u1", "k2", "m20", "m21",
     "m22", "m23", "k3", "m30", "m31", "m32", "m33",
 )
-AFTER = (
-    "P2", "u2", "P3", "u3", "v1",
-)
+AFTER = ("v1",)
+DURING = (("r2", "y2", "r3", "y3"), (), (), ())
+MIXED = ("u2", "v2", "u3", "v3")
 SIDES = 2
 CORES = 2
 PAIR = 2
@@ -594,7 +594,7 @@
         mix_near=pltpu.VMEM((nz, WINDOW, V_DIM), bf),
         mix_in=pltpu.VMEM((nz, WINDOW, V_DIM), bf),
         out_wx=pltpu.VMEM((V_DIM, n * width), bf),
-        part=pltpu.VMEM((WINDOW, slab), f32),
+        part=pltpu.VMEM((nz * WINDOW, slab), f32),
         result=pltpu.VMEM((count, n * width), bf),
         keep=pltpu.VMEM((nz, nz, count, slab), f32),
         core_out=pltpu.VMEM((nz, nz, count, slab), bf),
@@ -618,10 +618,10 @@
         ox_s=dma((1,)),
         ox_r=dma((nz, SIDES)),
         rc_s=dma((1,)),
-        rc_r=dma((nz, nz)),
+        rc_r=dma((nz,)),
         rx_s=dma((1,)),
         rx_r=dma((nz,)),
-        rz_s=dma((1,)),
+        rz_s=dma((nz, nz - 1)),
         rz_r=dma((nz, nz)),
         load=dma((8,)),
         store=dma((1,)),
@@ -960,6 +960,10 @@
             m.ox_r.at[step, side],
             device(z, y, nx, c),
         )
+
+    def out_y(step, arrival):
+        piece = m.out_w.at[:, out_columns(toward(step), y)]
+        return remote(piece, piece, m.f_s.at[OUT, toward(step)], arrival, device(z, ny, x, c))
 
     fresh = set()
 
@@ -998,6 +1002,10 @@
             pass_tokens(step)
         elif word[0] == "x":
             across_tokens(step)
+        elif word[0] == "r":
+            out_y(step, m.w_r.at[OUT, toward(step)]).wait_recv()
+        elif word[0] == "y":
+            out_y(step, m.f_r.at[OUT, toward(step)]).start()
         elif word[0] == "u":
             out_x(step, y).start()
         elif word[0] == "v":
@@ -1088,13 +1096,9 @@
             return (far, near, mate, z)[turn]
         return jnp.where(turn == 0, far, jnp.where(turn == 1, near, jnp.where(turn == 2, mate, z)))
 
-    def core_copy(turn, piece):
+    def core_copy(piece):
         return remote(
-            m.core_out.at[turn, piece],
-            m.core_in.at[turn, piece],
-            m.rc_s.at[0],
-            m.rc_r.at[turn, piece],
-            device(z, y, x, nc),
+            m.core_out.at[piece], m.core_in.at[piece], m.rc_s.at[0], m.rc_r.at[piece], device(z, y, x, nc)
         )
 
     def mix_copy(turn):
@@ -1107,13 +1111,13 @@
         return remote(
             m.z_out.at[turn, spot],
             m.z_in.at[slot, spot],
-            m.rz_s.at[0],
+            m.rz_s.at[spot, turn],
             m.rz_r.at[slot, spot],
             device(target_z, y, x, c),
         )
 
-    def half_rows(cc):
-        return pl.ds(pl.multiple_of(cc * count, count), count)
+    def half_rows(turn, cc):
+        return pl.ds(pl.multiple_of(turn * WINDOW + cc * count, count), count)
 
     def slab_columns(piece):
         return pl.ds(pl.multiple_of(toward(piece) * slab, slab), slab)
@@ -1125,18 +1129,20 @@
         for side in (y, ny):
             out_x(piece, side).wait_recv()
 
-    def emit(turn, piece):
+    def emit(piece):
         columns = slab_columns(piece)
-        m.part[...] = dot_nn(m.mix_near[turn], m.out_w[:, columns]) + dot_nn(
-            m.mix_in[turn], m.out_wx[:, columns]
-        )
-        m.core_out[turn, piece] = m.part[half_rows(nc), :].astype(bf)
-        core_copy(turn, piece).start()
-        m.keep[turn, piece] = m.part[half_rows(c), :]
+        rows = nz * WINDOW
+        m.part[...] = dot_nn(m.mix_near[...].reshape(rows, V_DIM), m.out_w[:, columns]) + dot_nn(
+            m.mix_in[...].reshape(rows, V_DIM), m.out_wx[:, columns]
+        )
+        for turn in range(nz):
+            m.core_out[piece, turn] = m.part[half_rows(turn, nc), :].astype(bf)
+        core_copy(piece).start()
+        for turn in range(nz):
+            m.keep[piece, turn] = m.part[half_rows(turn, c), :]
 
     def joined(turn, piece):
-        core_copy(turn, piece).wait_recv()
-        return m.keep[turn, piece] + m.core_in[turn, piece].astype(f32)
+        return m.keep[piece, turn] + m.core_in[piece, turn].astype(f32)
 
     def pass_sum(turn, piece):
         m.z_out[turn, toward(piece)] = joined(turn, piece).astype(bf)
@@ -1148,30 +1154,11 @@
         m.z_out[turn, toward(piece)] = merged.astype(bf)
         z_copy(turn, piece, home(turn), nz - 1).start()
 
-    def first_sums(turn, piece):
-        if turn < PAIR:
-            pl.when(outer)(lambda: pass_sum(turn, piece))
-        elif turn < nz - 1:
-            pass_sum(turn, piece)
-
-    early, late = (0, 1), (2, 3)
-
     def rounds(block):
-        for turn in range(nz + 1):
-            if turn < nz:
-                block(turn)
-            if turn == 0:
-                perform("v2")
-            if turn == 1:
-                perform("v3")
-                for piece in early:
-                    take_out(piece)
-            if turn > 0:
-                mix_copy(turn - 1).wait_recv()
-                for piece in early:
-                    emit(turn - 1, piece)
-                for piece in early:
-                    first_sums(turn - 1, piece)
+        for turn in range(nz):
+            block(turn)
+            for word in DURING[turn]:
+                perform(word)
 
     for word in AFTER:
         perform(word)
@@ -1272,16 +1259,52 @@
         for turn in range(PAIR):
             merge_sum(turn, piece)
 
-    for piece in early:
+    def crossing(piece, before=None):
+        def paced():
+            if before is not None:
+                sent(before)
+            for turn in range(PAIR):
+                pass_sum(turn, piece)
+
+        core_copy(piece).wait_recv()
+        pl.when(outer)(paced)
+
+    def sent(piece):
+        for turn in range(PAIR):
+            z_copy(turn, piece, mate, turn).wait_send()
+
+    def staying(piece):
+        pass_sum(nz - 2, piece)
+
+    def second_round(piece):
         pl.when(inside)(functools.partial(merge_sums, piece))
-    for piece in late:
+
+    def make(piece):
         take_out(piece)
-        for turn in range(nz):
-            emit(turn, piece)
-        for turn in range(nz):
-            first_sums(turn, piece)
-    for piece in late:
-        pl.when(inside)(functools.partial(merge_sums, piece))
+        emit(piece)
+
+    for turn in range(nz):
+        mix_copy(turn).wait_recv()
+    for word in MIXED:
+        perform(word)
+    make(0)
+    make(1)
+    crossing(0)
+    for piece in range(1, nz):
+        crossing(piece, piece - 1)
+        pl.when(inside)(functools.partial(staying, piece - 1))
+        second_round(piece - 1)
+        if piece + 1 < nz:
+            make(piece + 1)
+
+    def last_sums():
+        sent(nz - 1)
+        for piece in range(nz):
+            staying(piece)
+
+    pl.when(outer)(last_sums)
+    pl.when(inside)(functools.partial(staying, nz - 1))
+    second_round(nz - 1)
     for piece in range(nz):
         total = joined(nz - 1, piece)
         for slot in (nz - 2, nz - 1):
@@ -1291,17 +1314,20 @@
         m.result[:, columns] = total.astype(bf)
         pltpu.make_async_copy(m.result.at[:, columns], out_ref.at[:, columns], m.store.at[0]).start()
 
+    for step in range(PAIR, nz):
+        out_y(step, m.f_r.at[OUT, toward(step)]).wait_send()
     for copy, condition in started:
         if condition is None:
             copy.wait_send()
         else:
             pl.when(condition)(copy.wait_send)
     everything = device(z, y, x, nc)
-    remote(m.core_out, m.core_in, m.rc_s.at[0], m.rc_r.at[0, 0], everything).wait_send()
+    remote(m.core_out, m.core_in, m.rc_s.at[0], m.rc_r.at[0], everything).wait_send()
     remote(m.mix_far, m.mix_in, m.rx_s.at[0], m.rx_r.at[0], everything).wait_send()
     remote(m.out_w, m.out_wx, m.ox_s.at[0], m.ox_r.at[0, 0], everything).wait_send()
-    sums = m.z_out.at[0 : nz - 1]
-    remote(sums, sums, m.rz_s.at[0], m.rz_r.at[0, 0], everything).wait_send()
+    for piece in range(nz):
+        pl.when(inside)(functools.partial(sent, piece))
+        z_copy(nz - 2, piece, mate, nz - 2).wait_send()
     pltpu.make_async_copy(m.result, out_ref, m.store.at[0]).wait()
 
 

time: 95.2 us -> 89.8 us (0.943)
  Pallas kernels: 93.3 us -> 88 us
    pallas_call x1, Pallas kernels: 93.3 us -> 88 us  [layer(): pl.pallas_call(functools.partial(layer_kernel, n, n_tp, tuple(scratch)),...]
where the time goes in v4:
time: 89.8 us; the launch traced here: 89.6 us
  Pallas kernels  88 us (98%)
  local copies, waits for them, and re-layouts  1.67 us (2%)
    pallas_call x1, Pallas kernels, layer(): pl.pallas_call(functools.partial(layer_kernel, n, n_tp, tuple(scratch)),...  88 us

profile of v4, /device:TPU:0, one launch (start us, length us, event | category | flops | bytes accessed | tf_op | source)
XLA Modules:
  0.0 89.6 jit_solution(70912712800134833)
XLA Ops:
  0.0 88.0 %layer.1 = bf16[64,2048]{1,0:T(8,128)(2,1)} custom-call(bf16[64,2048]{1,0:T(8,128)(2,1)} %refs_0_.1, f32[1,2048]{1,0:T(1,128)} %bitcast.6, f32[2,256]{1,0:T(2,128)} %refs_2_.1, f32[1,8]{1,0:T(1,128)} %bitcast.7, bf16[256,256]{1,0:T(8,128)(2,1)} %refs_4_.1, bf16[256,256]{1,0:T(8,128)(2,1)} %refs_5_.1, bf16[256,512]{1,0:T(8,128)(2,1)} %refs_6_.1, ...), custom_call_target="tpu_custom_call" | custom-call | flops 4294967296 | bytes 16777216 | tf_op jit(solution)/shard_map/layer/pallas_call | solution.py:1339
  88.0 1.7 %copy.14 = bf16[64,2048]{1,0:T(8,128)(2,1)} copy(bf16[64,2048]{1,0:T(8,128)(2,1)} %layer.1) | data formatting | bytes 524288

commit v5 on v4

--- a/solution.py
+++ b/solution.py
@@ -519,7 +519,7 @@
     "m22", "m23", "k3", "m30", "m31", "m32", "m33",
 )
 AFTER = ("v1",)
-DURING = (("r2", "y2", "r3", "y3"), (), (), ())
+DURING = ("r2", "y2", "r3", "y3")
 MIXED = ("u2", "v2", "u3", "v3")
 SIDES = 2
 CORES = 2
@@ -590,8 +590,7 @@
         kv=pltpu.VMEM((4, nz, length + WINDOW, 2 * HEAD_DIM), bf),
         rim=pltpu.VMEM((nz, WINDOW, 2 * HEAD_DIM), bf),
         halo=pltpu.VMEM((nz, WINDOW, 2 * HEAD_DIM), bf),
-        mix_far=pltpu.VMEM((nz, WINDOW, V_DIM), bf),
-        mix_near=pltpu.VMEM((nz, WINDOW, V_DIM), bf),
+        mixes=pltpu.VMEM((2, nz, WINDOW, V_DIM), bf),
         mix_in=pltpu.VMEM((nz, WINDOW, V_DIM), bf),
         out_wx=pltpu.VMEM((V_DIM, n * width), bf),
         part=pltpu.VMEM((nz * WINDOW, slab), f32),
@@ -1103,7 +1102,7 @@
 
     def mix_copy(turn):
         return remote(
-            m.mix_far.at[turn], m.mix_in.at[turn], m.rx_s.at[0], m.rx_r.at[turn], device(z, y, nx, c)
+            m.mixes.at[0, turn], m.mix_in.at[turn], m.rx_s.at[0], m.rx_r.at[turn], device(z, y, nx, c)
         )
 
     def z_copy(turn, piece, target_z, slot):
@@ -1132,7 +1131,7 @@
     def emit(piece):
         columns = slab_columns(piece)
         rows = nz * WINDOW
-        m.part[...] = dot_nn(m.mix_near[...].reshape(rows, V_DIM), m.out_w[:, columns]) + dot_nn(
+        m.part[...] = dot_nn(m.mixes[1].reshape(rows, V_DIM), m.out_w[:, columns]) + dot_nn(
             m.mix_in[...].reshape(rows, V_DIM), m.out_wx[:, columns]
         )
         for turn in range(nz):
@@ -1154,11 +1153,9 @@
         m.z_out[turn, toward(piece)] = merged.astype(bf)
         z_copy(turn, piece, home(turn), nz - 1).start()
 
-    def rounds(block):
-        for turn in range(nz):
-            block(turn)
-            for word in DURING[turn]:
-                perform(word)
+    def between():
+        for word in DURING:
+            perform(word)
 
     for word in AFTER:
         perform(word)
@@ -1193,12 +1190,12 @@
             total = total * lax.rsqrt(jnp.mean(total * total, axis=-1, keepdims=True) + epsilon)
             return total.astype(bf)
 
-        def both_blocks(turn):
-            m.mix_far[turn] = finish_block(home(turn), nx)
+        for turn in range(nz):
+            m.mixes[0, turn] = finish_block(home(turn), nx)
             mix_copy(turn).start()
-            m.mix_near[turn] = finish_block(home(turn), x)
-
-        rounds(both_blocks)
+        between()
+        for turn in range(nz):
+            m.mixes[1, turn] = finish_block(home(turn), x)
         for zz in range(nz):
             state_copy(zz).wait_send()
 
@@ -1223,10 +1220,10 @@
             for zz in range(nz):
                 place(zz, 0, m.halo[jnp.maximum(zz - 1 + y, 0)])
 
-        pl.when(x == 1)(take_halo)
-        def attend_block(zz, xx, target):
+        def attend_block(turn, xx):
+            zz, slot = home(turn), x if xx == 1 else nx
             bias = m.bias[jnp.minimum(zz + y + xx, 1)]
-            where = pl.ds(pl.multiple_of(xx * WINDOW, WINDOW), 2 * WINDOW)
+            where = pl.ds(xx * WINDOW, 2 * WINDOW)
             rows = block_rows(zz, xx)
             first = lane_kv < HEAD_DIM
             for pair in range(heads // 2):
@@ -1243,16 +1240,15 @@
                 below = pltpu.roll(jnp.where(first, terms[1], terms[0]), HEAD_DIM, 1)
                 below = below + jnp.where(first, ends[0], ends[1])
                 mixed = jnp.where(first, terms[0], terms[1]) / below
-                target[:, lanes] = mixed.astype(bf)
-
-        def both_blocks(turn):
-            attend_block(home(turn), nx, m.mix_far.at[turn])
-            mix_copy(turn).start()
-            if turn == 0:
-                pl.when(x == 0)(take_halo)
-            attend_block(home(turn), x, m.mix_near.at[turn])
-
-        rounds(both_blocks)
+                m.mixes[slot, turn, :, lanes] = mixed.astype(bf)
+            pl.when(x != xx)(mix_copy(turn).start)
+
+        for turn in range(nz):
+            attend_block(turn, 1)
+        take_halo()
+        between()
+        for turn in range(nz):
+            attend_block(turn, 0)
         halo_copy.wait_send()
 
     def merge_sums(piece):
@@ -1323,7 +1319,7 @@
             pl.when(condition)(copy.wait_send)
     everything = device(z, y, x, nc)
     remote(m.core_out, m.core_in, m.rc_s.at[0], m.rc_r.at[0], everything).wait_send()
-    remote(m.mix_far, m.mix_in, m.rx_s.at[0], m.rx_r.at[0], everything).wait_send()
+    remote(m.mixes.at[0], m.mix_in, m.rx_s.at[0], m.rx_r.at[0], everything).wait_send()
     remote(m.out_w, m.out_wx, m.ox_s.at[0], m.ox_r.at[0, 0], everything).wait_send()
     for piece in range(nz):
         pl.when(inside)(functools.partial(sent, piece))

time: 89.8 us -> 89.5 us (level)
  no operation moved by 1% of the time
where the time goes in v5:
time: 89.5 us; the launch traced here: 89.4 us
  Pallas kernels  87.7 us (98%)
  local copies, waits for them, and re-layouts  1.67 us (2%)
    pallas_call x1, Pallas kernels, layer(): pl.pallas_call(functools.partial(layer_kernel, n, n_tp, tuple(scratch)),...  87.7 us

profile of v5, /device:TPU:0, one launch (start us, length us, event | category | flops | bytes accessed | tf_op | source)
XLA Modules:
  0.0 89.4 jit_solution(11012232900657776666)
XLA Ops:
  0.0 87.7 %layer.1 = bf16[64,2048]{1,0:T(8,128)(2,1)} custom-call(bf16[64,2048]{1,0:T(8,128)(2,1)} %refs_0_.1, f32[1,2048]{1,0:T(1,128)} %bitcast.6, f32[2,256]{1,0:T(2,128)} %refs_2_.1, f32[1,8]{1,0:T(1,128)} %bitcast.7, bf16[256,256]{1,0:T(8,128)(2,1)} %refs_4_.1, bf16[256,256]{1,0:T(8,128)(2,1)} %refs_5_.1, bf16[256,512]{1,0:T(8,128)(2,1)} %refs_6_.1, ...), custom_call_target="tpu_custom_call" | custom-call | flops 4294967296 | bytes 16777216 | tf_op jit(solution)/shard_map/layer/pallas_call | solution.py:1335
  87.7 1.7 %copy.14 = bf16[64,2048]{1,0:T(8,128)(2,1)} copy(bf16[64,2048]{1,0:T(8,128)(2,1)} %layer.1) | data formatting | bytes 524288
